TPU v7x, 256 devices: a whole 4x4x8 slice. The times are simulated.
256 devices in a mesh: sp: 64 (over z, x, core), tp: 4 (over y).
Axes of the slice: x: 4, y: 4, z: 8, core: 2. Of those that a mesh axis runs over, the one named last changes fastest.
Arguments:
- query_rows: bfloat16 [32768, 1024], P('sp', 'tp'), may hold values from -6 to 6
- key_rows: bfloat16 [32768, 1024], P('sp', 'tp'), may hold values from -6 to 6
- value_rows: bfloat16 [32768, 2048], P('sp', 'tp'), may hold values from -6 to 6
- out_gate_pre: bfloat16 [32768, 2048], P('sp', 'tp'), may hold values from -8 to 8
- input_gate_pre: float32 [4, 32768], P('tp', 'sp'), may hold values from -8 to 8
- forget_gate_pre: float32 [4, 32768], P('tp', 'sp'), may hold values from -26 to 26
- residual: bfloat16 [32768, 2048], P(('sp', 'tp')), may hold values from -6 to 6
- out_proj: bfloat16 [2048, 2048], P('tp'), may hold values from -0.125 to 0.125
- mix_gain: float32 [2048], replicated, may hold values from 0.1 to 1.9
- pre_gain: float32 [2048], replicated, may hold values from 0.1 to 1.9
- gate_proj: bfloat16 [2048, 3072], P('sp', 'tp'), may hold values from -0.125 to 0.125
- value_proj: bfloat16 [2048, 3072], P('sp', 'tp'), may hold values from -0.125 to 0.125
- gate_kernel: float32 [3, 3072], P(None, 'tp'), may hold values from -3.5 to 3.5
- value_kernel: float32 [3, 3072], P(None, 'tp'), may hold values from -3.5 to 3.5
- down_proj: bfloat16 [2048, 3072], P('sp', 'tp'), may hold values from -0.109375 to 0.109375
- post_gain: float32 [2048], replicated, may hold values from 0.1 to 1.9
Outputs:
- result: bfloat16 [32768, 2048], P(('sp', 'tp'))
All inputs are finite; a program needn't handle non-finite values.
Results may differ from a plain program's by a relative error of at most 0.017.
Values may be sent and summed in bfloat16 or wider, within the bound.
A program may use at most 128 MiB of HBM per device.

v0:
```python
import jax
import jax.numpy as jnp
from jax import lax
from jax.sharding import Mesh
from jax.sharding import PartitionSpec as P

QK = 256
HV = 512
BLOCK = 64
CONV = 3
SP = ("sp_0", "sp_1", "sp_2")
SP_TP = ("sp_0", "sp_1", "sp_2", "tp")


gate_cap = 15.0
epsilon = 1e-06
highest = lax.Precision.HIGHEST
far_below = -1e30


def sent_together(arrays, axis, dim, along):
    widths = [a.shape[along] for a in arrays]
    both = jnp.concatenate(arrays, axis=along)
    whole = lax.all_gather(both, axis, axis=dim, tiled=True)
    return tuple(jnp.split(whole, [sum(widths[:k]) for k in range(1, len(widths))], axis=along))


def filled_with(shard, identity):
    return jax.tree.map(
        lambda a, e: jnp.broadcast_to(jnp.asarray(e, a.dtype), a.shape), shard, identity
    )


def all_in_one(shard, axis):
    leaves = jax.tree.leaves(shard)
    order = sorted(range(len(leaves)), key=lambda k: -leaves[k].size)
    width = (1, *leaves[order[0]].shape)[-1]
    lines = [
        jnp.pad(leaves[k].reshape(-1), (0, -leaves[k].size % width)).reshape(-1, width)
        for k in order
    ]
    both, at, found = (lax.all_gather(jnp.concatenate(lines), axis), 0, {})
    for k, line in zip(order, lines):
        piece = both[:, at : at + len(line)].reshape(len(both), -1)
        found[k] = piece[:, : leaves[k].size].reshape(-1, *leaves[k].shape)
        at += len(line)
    numbers = iter(range(len(leaves)))
    return jax.tree.map(lambda _: found[next(numbers)], shard)


def prefix_by_axis(shard, axes, combine, identity):
    before = start = filled_with(shard, identity)
    so_far = shard
    for axis in reversed(axes):
        devices, mine = (lax.axis_size(axis), lax.axis_index(axis))
        pieces = all_in_one(so_far, axis)
        inside, so_far = (start, start)
        for k in range(devices):
            passed = k < mine
            so_far = combine(so_far, jax.tree.map(lambda part: part[k], pieces))
            inside = jax.tree.map(lambda new, old: jnp.where(passed, new, old), so_far, inside)
        before = combine(inside, before)
    return before


def in_blocks(shard, dim, devices):
    shape = shard.shape
    blocks = shard.reshape(*shape[:dim], devices, shape[dim] // devices, *shape[dim + 1 :])
    return jnp.moveaxis(blocks, dim, 0)


def sum_at_owner(shard, axis, dim):
    blocks = in_blocks(shard, dim, lax.axis_size(axis))
    arrived = lax.all_to_all(blocks, axis, split_axis=0, concat_axis=0, tiled=True)
    return arrived.astype(jnp.float32).sum(axis=0)


def joined_along(blocks, dim):
    shape = list(blocks.shape[1:])
    shape[dim] *= blocks.shape[0]
    return jnp.moveaxis(blocks, 0, dim).reshape(shape)


def from_everyone(shard, axis):
    copies = jnp.broadcast_to(shard, (lax.axis_size(axis), *shard.shape))
    return lax.all_to_all(copies, axis, split_axis=0, concat_axis=0, tiled=True)


def gather_directly(shard, axis, dim):
    return joined_along(from_everyone(shard, axis), dim)


def passed_along(block, axis, distance):
    devices = range(lax.axis_size(axis))
    route = [(i - distance, i) for i in devices if i - distance in devices]
    return lax.ppermute(block, axis, route)


def softcap(values):
    return gate_cap * jnp.tanh(values / gate_cap)


def normalize(values, gains):
    return values * lax.rsqrt(jnp.mean(values * values, axis=-1, keepdims=True) + epsilon) * gains


def combine(previous, following):
    prev_total, prev_max, prev_memory, prev_normer = previous
    next_total, next_max, next_memory, next_normer = following
    new_max = jnp.maximum(next_total + prev_max, next_max)
    prev_scale = jnp.exp(next_total + prev_max - new_max)
    next_scale = jnp.exp(next_max - new_max)
    memory = prev_scale[..., None, None] * prev_memory + next_scale[..., None, None] * next_memory
    normer = prev_scale[..., None] * prev_normer + next_scale[..., None] * next_normer
    return (prev_total + next_total, new_max, memory, normer)


def depthwise(padded, kernel, length):
    summed = kernel[0] * padded[0:length]
    for offset in range(1, CONV):
        summed = summed + kernel[offset] * padded[offset : offset + length]
    return summed


def body(
    query_rows,
    key_rows,
    value_rows,
    out_gate_pre,
    input_gate_pre,
    forget_gate_pre,
    residual,
    out_proj,
    mix_gain,
    pre_gain,
    gate_proj,
    value_proj,
    gate_kernel,
    value_kernel,
    down_proj,
    post_gain,
):
    row_count = query_rows.shape[0]
    head_count = input_gate_pre.shape[0]
    blocks = row_count // BLOCK
    hidden_width = gate_proj.shape[1]
    full_gate, full_value, full_down = sent_together((gate_proj, value_proj, down_proj), SP, 0, 1)
    query_scale = QK ** (-0.5)
    query_narrow = (
        (query_rows * jnp.bfloat16(query_scale))
        .reshape(blocks, BLOCK, head_count, QK)
        .transpose(2, 0, 1, 3)
    )
    key_narrow = key_rows.reshape(blocks, BLOCK, head_count, QK).transpose(2, 0, 1, 3)
    queries = query_narrow.astype(jnp.float32)
    key_blocks = key_narrow.astype(jnp.float32)
    value_blocks = (
        value_rows.astype(jnp.float32).reshape(blocks, BLOCK, head_count, HV).transpose(2, 0, 1, 3)
    )
    log_input = softcap(input_gate_pre).reshape(head_count, blocks, BLOCK)
    log_forget = jax.nn.log_sigmoid(softcap(forget_gate_pre)).reshape(head_count, blocks, BLOCK)
    running = jnp.cumsum(log_forget, axis=2)
    block_total = running[..., -1]
    lead_logs = block_total[..., None] - running + log_input
    lead_max = jnp.max(lead_logs, axis=2)
    weighted = key_blocks * jnp.exp(lead_logs - lead_max[..., None])[..., None]
    block_memory = jnp.einsum("hbsd,hbsv->hbdv", weighted, value_blocks, precision=highest)
    segments = (block_total, lead_max, block_memory, jnp.sum(weighted, axis=2))
    inclusive = lax.associative_scan(combine, segments, axis=1)
    summary = tuple((member[:, -1] for member in inclusive))
    identity = (
        jnp.zeros((head_count,), jnp.float32),
        jnp.full((head_count,), far_below, jnp.float32),
        jnp.zeros((head_count, QK, HV), jnp.float32),
        jnp.zeros((head_count, QK), jnp.float32),
    )
    incoming = prefix_by_axis(summary, SP, combine, identity)
    exclusive = tuple(
        (
            jnp.concatenate((start_member[:, None], member[:, :-1]), axis=1)
            for start_member, member in zip(identity, inclusive)
        )
    )
    entering = combine(tuple((member[:, None] for member in incoming)), exclusive)
    causal = jnp.tril(jnp.ones((BLOCK, BLOCK), dtype=bool))
    log_weights = jnp.where(
        causal, running[..., :, None] - running[..., None, :] + log_input[..., None, :], -jnp.inf
    )
    carried = running + entering[1][..., None]
    row_max = jnp.maximum(carried, jnp.max(log_weights, axis=3))
    inner_weights = jnp.exp(log_weights - row_max[..., None])
    outer_weights = jnp.exp(carried - row_max)
    scores = (
        jnp.einsum("hbtd,hbsd->hbts", query_narrow, key_narrow, preferred_element_type=jnp.float32)
        * inner_weights
    )
    numerator = outer_weights[..., None] * jnp.einsum(
        "hbtd,hbdv->hbtv", queries, entering[2], precision=highest
    ) + jnp.einsum("hbts,hbsv->hbtv", scores, value_blocks, precision=highest)
    denominator = outer_weights * jnp.einsum(
        "hbtd,hbd->hbt", queries, entering[3], precision=highest
    ) + jnp.sum(scores, axis=3)
    cell_rows = numerator / jnp.maximum(jnp.abs(denominator), jnp.exp(-row_max))[..., None]
    cell_rows = cell_rows.transpose(1, 2, 0, 3).reshape(row_count, head_count * HV)
    gated = (cell_rows * jax.nn.sigmoid(out_gate_pre.astype(jnp.float32))).astype(jnp.bfloat16)
    rows_part = gated
    mixed = sum_at_owner(
        jnp.dot(rows_part, out_proj, preferred_element_type=jnp.float32).astype(jnp.bfloat16),
        "tp",
        0,
    ).astype(jnp.bfloat16)
    stream = (residual.astype(jnp.float32) + normalize(mixed.astype(jnp.float32), mix_gain)).astype(
        jnp.bfloat16
    )
    normed = normalize(stream.astype(jnp.float32), pre_gain).astype(jnp.bfloat16)
    shard_rows = gather_directly(normed, "tp", 0)
    gate_part = jnp.dot(shard_rows, full_gate, preferred_element_type=jnp.float32).astype(
        jnp.bfloat16
    )
    value_part = jnp.dot(shard_rows, full_value, preferred_element_type=jnp.float32).astype(
        jnp.bfloat16
    )
    up_both = jnp.concatenate((gate_part, value_part), axis=1)
    up_gate = up_both[:, :hidden_width]
    up_value = up_both[:, hidden_width:]
    last_rows = jnp.concatenate(
        (up_gate[row_count - CONV + 1 :], up_value[row_count - CONV + 1 :]), axis=1
    )
    before = passed_along(last_rows, SP, 1)
    gate_padded = jnp.concatenate((before[:, :hidden_width], up_gate), axis=0).astype(jnp.float32)
    value_padded = jnp.concatenate((before[:, hidden_width:], up_value), axis=0).astype(jnp.float32)
    conv_gate = depthwise(gate_padded, gate_kernel, row_count)
    conv_value = depthwise(value_padded, value_kernel, row_count)
    hidden = (jax.nn.silu(conv_gate) * conv_value).astype(jnp.bfloat16)
    rows_part = hidden
    ffn = sum_at_owner(
        lax.dot_general(
            rows_part, full_down, (((1,), (1,)), ((), ())), preferred_element_type=jnp.float32
        ).astype(jnp.bfloat16),
        "tp",
        0,
    ).astype(jnp.bfloat16)
    return (stream.astype(jnp.float32) + normalize(ffn.astype(jnp.float32), post_gain)).astype(
        jnp.bfloat16
    )


def solution(mesh):
    finer = Mesh(mesh.devices.reshape(8, 4, 2, mesh.shape["tp"]), ("sp_0", "sp_1", "sp_2", "tp"))
    placed = (
        P(SP, "tp"),
        P(SP, "tp"),
        P(SP, "tp"),
        P(SP, "tp"),
        P("tp", SP),
        P("tp", SP),
        P(SP_TP, None),
        P("tp", None),
        P(),
        P(),
        P(SP, "tp"),
        P(SP, "tp"),
        P(None, "tp"),
        P(None, "tp"),
        P(SP, "tp"),
        P(),
    )
    return jax.shard_map(
        body, mesh=finer, in_specs=placed, out_specs=P(SP_TP, None), check_vma=False
    )
```

profile of v0, /device:TPU:2, one launch (start us, length us, event | category | flops | bytes accessed | tf_op | source)
XLA Modules:
  0.0 350.6 jit_solution(6190709636447441226)
XLA Ops:
  6.5 0.9 fusion.85
  8.6 1.3 fusion.117
  18.1 1.1 fusion.76
  19.2 3.3 convolution_bitcast_fusion
  22.6 2.3 multiply_add_fusion
  25.5 1.8 multiply_add_fusion.1
  27.7 1.4 copy-done.4
  29.0 1.2 fusion.120
  30.3 2.3 pad_maximum_fusion.1
  32.5 3.4 pad.119
  35.9 2.4 pad.120
  38.3 4.1 %add.620 = f32[1,4,256,512]{3,2,1,0:T(8,128)} add(f32[1,4,256,512]{3,2,1,0:T(8,128)} %pad.119, f32[1,4,256,512]{3,2,1,0:T(8,128)} %pad.120) | non-fusion elementwise | flops 524288 | bytes 6291456 | tf_op jit(solution)/shard_map/add | solution.py:169
  42.4 5.7 %pad.274 = f32[1,8,256,512]{3,2,1,0:T(8,128)} pad(f32[1,4,256,512]{3,2,1,0:T(8,128)} %add.620, f32[]{:T(128)} %constant.87.clone.1), padding=0_0_0x1_0_1x0_0_0x0_0_0 | pad | bytes 6291460
  50.1 0.8 pad_add_fusion.3
  52.6 3.0 fusion.24
  55.6 1.6 pad_maximum_fusion
  57.1 5.7 %pad.121 = f32[1,8,256,512]{3,2,1,0:T(8,128)} pad(f32[1,4,256,512]{3,2,1,0:T(8,128)} %pad_maximum_fusion, f32[]{:T(128)} %constant.87.clone.1), padding=0_0_0x0_1_1x0_0_0x0_0_0 | pad | bytes 6291460 | tf_op jit(solution)/shard_map/pad | solution.py:169
  65.9 1.3 add_bitcast_fusion
  67.2 0.9 maximum_bitcast_fusion
  68.1 17.5 %all-gather.13.cloned.1.call-done = f32[2,259,512]{2,1,0:T(8,128)} async-done(((f32[1,259,512]{2,1,0:T(8,128)}), f32[2,259,512]{2,1,0:T(8,128)}) %all-gather.13.cloned.1.call-update) | async-done | bytes 1060880 | tf_op jit(solution)/shard_map/all_gather | solution.py:42
  85.6 0.9 fusion.121
  93.0 1.3 fusion.80
  94.3 0.9 maximum_bitcast_fusion.1
  95.3 34.3 %all-gather.15.cloned.1.call-done = f32[4,259,512]{2,1,0:T(8,128)} async-done(((f32[1,259,512]{2,1,0:T(8,128)}), f32[4,259,512]{2,1,0:T(8,128)}) %all-gather.15.cloned.1.call-update) | async-done | bytes 2121744 | tf_op jit(solution)/shard_map/all_gather | solution.py:42
  129.6 1.0 fusion.119
  142.3 1.8 fusion.149
  144.2 0.9 maximum_bitcast_fusion.2
  146.1 5.6 %pad.185 = f32[1,7,256,512]{3,2,1,0:T(8,128)} pad(f32[1,4,256,512]{3,2,1,0:T(8,128)} %pad_maximum_fusion, f32[]{:T(128)} %constant.87.clone.1), padding=0_0_0x0_0_1x0_0_0x0_0_0 | pad | bytes 5767172 | tf_op jit(solution)/shard_map/slice | solution.py:180
  152.1 0.7 broadcast_multiply_fusion
  152.9 5.9 %slice_add_fusion.3 = f32[1,7,256,512]{3,2,1,0:T(8,128)} fusion(f32[1,7,256,512]{3,2,1,0:T(8,128)} %pad.185, f32[1,8,256,512]{3,2,1,0:T(8,128)} %pad.274), kind=kLoop, calls=%fused_computation.265 | loop fusion | flops 917504 | bytes 11010048 | tf_op jit(solution)/shard_map/add | solution.py:169
  160.3 41.9 %all-gather.17.cloned.1.call-done = f32[8,259,512]{2,1,0:T(8,128)} async-done(((f32[1,259,512]{2,1,0:T(8,128)}), f32[8,259,512]{2,1,0:T(8,128)}) %all-gather.17.cloned.1.call-update) | async-done | bytes 4243472 | tf_op jit(solution)/shard_map/all_gather | solution.py:42
  202.2 1.1 fusion.118
  220.2 1.3 fusion.81
  221.5 1.2 fusion.137
  222.8 4.1 %fusion.61 = f32[256,512]{1,0:T(8,128)S(1)} fusion(f32[8,259,512]{2,1,0:T(8,128)} %all-gather.17.cloned.1.call-done, f32[2,259,512]{2,1,0:T(8,128)S(1)} %copy-done.5, f32[4,259,512]{2,1,0:T(8,128)} %all-gather.15.cloned.1.call-done, f32[]{:T(128)} %bitcast.117, f32[]{:T(128)} %bitcast.116, f32[]{:T(128)} %bitcast.115, f32[]{:T(128)} %bitcast.114, ...), kind=kLoop, calls=%fused_computation.84 | loop fusion | flops 7995392 | bytes 7864470 | tf_op jit(solution)/shard_map/mul | solution.py:113
  226.9 2.2 fusion.32
  230.4 1.3 convolution_convert_fusion
  231.7 30.3 %all_to_all.15 = bf16[4,128,2048]{2,1,0:T(8,128)(2,1)S(1)} all-to-all(bf16[4,128,2048]{2,1,0:T(8,128)(2,1)S(1)} %bitcast.204), channel_id=1, replica_groups=mesh['sp_0'=8,'sp_1'=4,'sp_2'=2,'tp'=4] {'tp'}, dimensions={0} | all-to-all | bytes 4194304 | tf_op jit(solution)/shard_map/all_to_all | solution.py:74
  262.7 1.4 fusion.41
  264.6 28.6 %all_to_all.16 = bf16[4,128,2048]{2,1,0:T(8,128)(2,1)} all-to-all(bf16[4,128,2048]{2,1,0:T(8,128)(2,1)S(1)} %broadcast_in_dim.23), channel_id=1, replica_groups=mesh['sp_0'=8,'sp_1'=4,'sp_2'=2,'tp'=4] {'tp'}, dimensions={0} | all-to-all | bytes 4194304 | tf_op jit(solution)/shard_map/all_to_all | solution.py:86
  293.2 4.5 %fusion.25 = bf16[512,768]{1,0:T(8,128)(2,1)S(1)} fusion(bf16[512,2048]{1,0:T(8,128)(2,1)} %bitcast.202, bf16[2048,2304]{1,0:T(8,128)(2,1)} %all-gather.11.cloned.1.call-done), kind=kOutput, calls=%fused_computation.37 | convolution fusion | flops 1611005952 | bytes 6029312 | tf_op jit(solution)/shard_map/dot_general | solution.py:217
  297.7 3.7 %fusion.28 = bf16[512,768]{1,0:T(8,128)(2,1)S(1)} fusion(bf16[512,2048]{1,0:T(8,128)(2,1)S(1)} %bitcast.203, bf16[2048,2304]{1,0:T(8,128)(2,1)} %all-gather.11.cloned.1.call-done), kind=kOutput, calls=%fused_computation.38 | convolution fusion | flops 1611005952 | bytes 6029312 | tf_op jit(solution)/shard_map/dot_general | solution.py:220
  301.4 2.1 collective-permute-start
  303.7 2.7 collective-permute-done
  306.7 4.6 %fusion.12 = bf16[512,2048]{1,0:T(8,128)(2,1)S(1)} fusion(bf16[2048,2304]{1,0:T(8,128)(2,1)} %all-gather.11.cloned.1.call-done, f32[514,768]{1,0:T(8,128)S(1)} %maximum_convert_fusion.1, f32[514,768]{1,0:T(8,128)S(1)} %maximum_convert_fusion, f32[768]{0:T(1024)S(1)} %get-tuple-element.9, f32[768]{0:T(1024)S(1)} %get-tuple-element.10, ...), kind=kOutput, calls=%fused_computation.12 | convolution fusion | flops 1617952768 | bytes 14704640 | tf_op jit(solution)/shard_map/dot_general | solution.py:237
  311.3 29.4 %all_to_all.17 = bf16[4,128,2048]{2,1,0:T(8,128)(2,1)} all-to-all(bf16[4,128,2048]{2,1,0:T(8,128)(2,1)S(1)} %bitcast.201), channel_id=1, replica_groups=mesh['sp_0'=8,'sp_1'=4,'sp_2'=2,'tp'=4] {'tp'}, dimensions={0} | all-to-all | bytes 4194304 | tf_op jit(solution)/shard_map/all_to_all | solution.py:74
  340.8 2.0 reduce_sum.77
  343.0 1.1 fusion.44
  (177 shorter events, 19.1 us)
Async XLA Ops:
  6.5 223.9 %copy-start = (bf16[512,2048]{1,0:T(8,128)(2,1)S(1)}, bf16[512,2048]{1,0:T(8,128)(2,1)}, u32[]{:S(2)}) copy-start(bf16[512,2048]{1,0:T(8,128)(2,1)} %param.23) | copy-start | bytes 6291460
  6.5 79.1 %all-gather.13.cloned.1.call-start = ((), (), s32[]{:S(2)}) async-start(), calls=%async_computation.4 | async-start | bytes 1622016 | tf_op jit(solution)/shard_map/all_gather | solution.py:42
  22.6 2.7 copy-start.2
  27.5 1.6 copy-start.4
  52.6 3.0 slice-start
  68.1 61.5 %all-gather.15.cloned.1.call-start = ((), (), s32[]{:S(2)}) async-start(), calls=%async_computation.5 | async-start | bytes 2703360 | tf_op jit(solution)/shard_map/all_gather | solution.py:42
  95.2 107.0 %all-gather.17.cloned.1.call-start = ((), (), s32[]{:S(2)}) async-start(), calls=%async_computation.6 | async-start | bytes 4866048 | tf_op jit(solution)/shard_map/all_gather | solution.py:42
  142.3 3.0 copy-start.12
  142.3 3.0 copy-start.13
  142.3 3.0 copy-start.14
  145.1 148.1 %all-gather.11.cloned.1.call-start = ((), (), s32[]{:S(2)}) async-start(), calls=%async_computation.3 | async-start | bytes 9584640 | tf_op jit(solution)/shard_map/all_gather | solution.py:24
  146.0 6.1 %copy-start.11 = (bf16[512,256]{1,0:T(8,128)(2,1)S(1)}, bf16[512,256]{1,0:T(8,128)(2,1)}, u32[]{:S(2)}) copy-start(bf16[512,256]{1,0:T(8,128)(2,1)} %param.16) | copy-start | bytes 786436
  152.9 68.6 %copy-start.7 = (bf16[512,256]{1,0:T(8,128)(2,1)S(1)}, bf16[512,256]{1,0:T(8,128)(2,1)}, u32[]{:S(2)}) copy-start(bf16[512,256]{1,0:T(8,128)(2,1)} %param.17) | copy-start | bytes 786436
  158.7 64.0 %copy-start.5 = (f32[2,259,512]{2,1,0:T(8,128)S(1)}, f32[2,259,512]{2,1,0:T(8,128)}, u32[]{:S(2)}) copy-start(f32[2,259,512]{2,1,0:T(8,128)} %all-gather.13.cloned.1.call-done) | copy-start | bytes 3182596
  222.8 4.1 %copy-start.3 = (f32[1,7,256,512]{3,2,1,0:T(8,128)S(1)}, f32[1,7,256,512]{3,2,1,0:T(8,128)}, u32[]{:S(2)}) copy-start(f32[1,7,256,512]{3,2,1,0:T(8,128)} %slice_add_fusion.3) | copy-start | bytes 11010052
  222.8 4.1 %copy-start.8 = (bf16[512,256]{1,0:T(8,128)(2,1)S(1)}, bf16[512,256]{1,0:T(8,128)(2,1)}, u32[]{:S(2)}) copy-start(bf16[512,256]{1,0:T(8,128)(2,1)} %broadcast_multiply_fusion) | copy-start | bytes 786436
  226.9 2.2 copy-start.10
  229.1 1.0 copy-start.9
  262.0 0.7 copy-start.15
  262.0 2.2 copy-start.16
  293.2 4.5 %copy-start.6 = (bf16[4,128,2048]{2,1,0:T(8,128)(2,1)S(1)}, bf16[4,128,2048]{2,1,0:T(8,128)(2,1)}, u32[]{:S(2)}) copy-start(bf16[4,128,2048]{2,1,0:T(8,128)(2,1)} %all_to_all.16) | copy-start | bytes 6291460
  297.7 5.9 %copy-start.18 = (f32[3,768]{1,0:T(4,128)S(1)}, f32[3,768]{1,0:T(4,128)}, u32[]{:S(2)}) copy-start(f32[3,768]{1,0:T(4,128)} %param.29) | copy-start | bytes 27652
  297.7 5.9 %copy-start.19 = (f32[3,768]{1,0:T(4,128)S(1)}, f32[3,768]{1,0:T(4,128)}, u32[]{:S(2)}) copy-start(f32[3,768]{1,0:T(4,128)} %param.28) | copy-start | bytes 27652
  301.4 4.9 %collective-permute-start = (bf16[2,1536]{1,0:T(2,128)(2,1)S(1)}, bf16[2,1536]{1,0:T(2,128)(2,1)S(1)}, u32[]{:S(2)}, u32[]{:S(2)}) collective-permute-start(bf16[2,1536]{1,0:T(2,128)(2,1)S(1)} %pad_maximum_fusion.3), channel_id=1, source_target_pairs={{0,4},{4,8},{8,12},{12,16},{16,20},{20,24},{24,28},{28,32},{32,36}... | collective-permute-start | bytes 18440 | tf_op jit(solution)/shard_map/ppermute | solution.py:96
  311.3 32.7 %copy-start.1 = (bf16[512,2048]{1,0:T(8,128)(2,1)S(1)}, bf16[512,2048]{1,0:T(8,128)(2,1)}, u32[]{:S(2)}) copy-start(bf16[512,2048]{1,0:T(8,128)(2,1)} %param.23) | copy-start | bytes 6291460
  340.7 2.2 copy-start.17
Sparse Core Ops, SparseCore 0:
  68.2 17.3 all-gather.12
  95.3 34.1 all-gather.14
  145.2 56.9 all-gather.16
  204.8 81.4 all-gather.10
where the time goes:
time: 352 us; the launch traced here: 351 us
  waiting for transfers between devices  96.4 us (27%)
  blocking collectives  88.3 us (25%)
  between operations  53 us (15%)
  other arithmetic  48.6 us (14%)
  local copies, waits for them, and re-layouts  39.1 us (11%)
  matrix products  22.7 us (6%)
    all_gather x3, waiting for transfers between devices, all_in_one(): both, at, found = (lax.all_gather(jnp.concatenate(lines), axis), 0, {})  93.7 us
    all_to_all x2, blocking collectives, sum_at_owner(): lax.all_to_all(blocks, axis, split_axis=0, concat_axis=0, tiled=True)  59.7 us
    all_to_all x1, blocking collectives, from_everyone(): return lax.all_to_all(copies, axis, split_axis=0, concat_axis=0, tiled=True)  28.6 us
    pad x15, local copies, waits for them, and re-layouts, body(): inclusive = lax.associative_scan(combine, segments, axis=1)  12.2 us
    add x13, other arithmetic, body(): inclusive = lax.associative_scan(combine, segments, axis=1)  11.4 us
    unnamed x50, local copies, waits for them, and re-layouts  8.03 us
    add x4, other arithmetic, combine(): prev_scale[..., None, None] * prev_memory  7.2 us
  transfers between devices with their start and end apart: 5, of which 4 were waited for; matrix products, arithmetic and copies ran while one was open for 8% of the time, Pallas kernels for 0%

commit v1 on v0

v1 whole, which is shorter than its diff:
```python
import functools

import jax
import jax.numpy as jnp
from jax import lax
from jax.experimental import pallas as pl
from jax.experimental.pallas import tpu as pltpu
from jax.sharding import PartitionSpec as P

f32 = jnp.float32
bf16 = jnp.bfloat16
MESH = pl.DeviceIdType.MESH

gate_cap = 15.0
epsilon = 1e-06
far_below = -1e30
CONV = 3
LANES = 128
ROW_STEP = 64
NORM_STEP = 16
CONV_STEP = 32
TILE = 256

SHAPES = {64: (8, 4, 2)}


def softcap(values):
    return gate_cap * jnp.tanh(values * (1.0 / gate_cap))


def log_one_plus(values):
    series = values * (
        1.0 + values * (-1 / 2 + values * (1 / 3 + values * (-1 / 4 + values * (1 / 5))))
    )
    return jnp.where(values < 0.015625, series, jnp.log(1.0 + values))


def log_sigmoid(values):
    return jnp.minimum(values, 0.0) - log_one_plus(jnp.exp(-jnp.abs(values)))


def normalize(values, gains):
    return values * lax.rsqrt(jnp.mean(values * values, axis=-1, keepdims=True) + epsilon) * gains


def matmul(left, right, left_dim=1, right_dim=0):
    return lax.dot_general(
        left, right, (((left_dim,), (right_dim,)), ((), ())), preferred_element_type=f32
    )


def mod(value, size):
    return lax.rem(value + size, jnp.int32(size))


def kernel(
    Z, X, C, T,
    q_ref, k_ref, v_ref, og_ref, ig_ref, fg_ref, res_ref, mixg_ref, preg_ref, postg_ref,
    gk_ref, vk_ref, outp_ref, gatep_ref, valuep_ref, downp_ref,
    out_ref,
    msend, mrecv, st_src, st_recv, ssend, srecv, nin, m_in, kwb, runc, a1, m1, d1,
    gsend, grecv, wo, wu, wd, rows_all, mixed, stream, upb, hidden, pbuf, from_left, from_right,
    relay_top, relay_bot,
    loc, p1, p2, xs, xd, zs, zd, wos, wod, ags, rss, a2, halo,
):
    NSP = Z * X * C
    rows, qk = q_ref.shape
    hv = v_ref.shape[1]
    own, D = out_ref.shape
    ffd = gatep_ref.shape[1]
    scale = float(qk) ** -0.5
    me = lax.axis_index("sp")
    tp = lax.axis_index("tp")
    core = lax.rem(me, jnp.int32(C))
    xx = lax.rem(lax.div(me, jnp.int32(C)), jnp.int32(X))
    zz = lax.div(me, jnp.int32(C * X))
    pending = []

    def at_sp(index):
        return {"sp": index, "tp": tp}

    def at_tp(index):
        return {"sp": me, "tp": index}

    def send(src, dst, ssem, rsem, device):
        copy = pltpu.make_async_remote_copy(
            src_ref=src, dst_ref=dst, send_sem=ssem, recv_sem=rsem,
            device_id=device, device_id_type=MESH,
        )
        copy.start()
        pending.append(copy)

    def arrived(dst, ssem, rsem, device):
        pltpu.make_async_remote_copy(
            src_ref=dst, dst_ref=dst, send_sem=ssem, recv_sem=rsem,
            device_id=device, device_id_type=MESH,
        ).wait_recv()

    def ds(start, size, step=None):
        return pl.ds(pl.multiple_of(start, step or size), size)

    sibling = at_sp(me + 1 - 2 * core) if C == 2 else None

    barrier = pltpu.get_barrier_semaphore()

    def greet(p, carry):
        pl.semaphore_signal(
            barrier, 1, device_id=at_sp(mod(me + p, NSP)), device_id_type=MESH
        )
        return carry

    lax.fori_loop(1, NSP, greet, 0)
    for k in range(1, T):
        pl.semaphore_signal(barrier, 1, device_id=at_tp(mod(tp + k, T)), device_id_type=MESH)

    shard = gatep_ref.shape[0]
    wrows = outp_ref.shape[0]
    mine = ds(me * shard, shard)
    local = [
        pltpu.make_async_copy(gatep_ref, wu.at[mine, pl.ds(0, ffd)], loc.at[0]),
        pltpu.make_async_copy(valuep_ref, wu.at[mine, pl.ds(ffd, ffd)], loc.at[1]),
        pltpu.make_async_copy(downp_ref, wd.at[mine], loc.at[2]),
        pltpu.make_async_copy(outp_ref, wo.at[ds(tp * wrows, wrows)], loc.at[3]),
    ]
    for copy in local:
        copy.start()

    steps = rows // ROW_STEP
    lane = lax.broadcasted_iota(jnp.int32, (ROW_STEP, rows), 1)
    line = lax.broadcasted_iota(jnp.int32, (ROW_STEP, rows), 0)
    li_row = softcap(ig_ref[...])
    lf_row = log_sigmoid(softcap(fg_ref[...]))

    def sums(b, run_row):
        here = line + b * ROW_STEP
        run_col = jnp.sum(jnp.where(lane <= here, lf_row, 0.0), axis=1, keepdims=True)
        runc[ds(b * ROW_STEP, ROW_STEP), :] = run_col
        return run_row + jnp.sum(jnp.where(lane == here, run_col, 0.0), axis=0, keepdims=True)

    run_row = lax.fori_loop(0, steps, sums, jnp.zeros((1, rows), f32))
    total = run_row[:, rows - 1 : rows]
    lead = total - run_row + li_row
    lead_max = jnp.max(lead, axis=1, keepdims=True)
    lead_weights = jnp.exp(lead - lead_max)

    def weigh(b, normer):
        here = line + b * ROW_STEP
        at = ds(b * ROW_STEP, ROW_STEP)
        column = jnp.sum(jnp.where(lane == here, lead_weights, 0.0), axis=1, keepdims=True)
        weighted = k_ref[at, :].astype(f32) * column
        kwb[at, :] = weighted.astype(bf16)
        return normer + jnp.sum(weighted, axis=0, keepdims=True)

    normer = lax.fori_loop(0, steps, weigh, jnp.zeros((1, qk), f32))
    nq = qk // LANES
    for r in range(nq):
        st_src[r : r + 1, :] = normer[:, r * LANES : (r + 1) * LANES]
    for r in range(nq, 4):
        st_src[r : r + 1, :] = jnp.broadcast_to(total if r == nq else lead_max, (1, LANES))
    R = msend.shape[1]
    nc = hv // LANES
    for r in range(nq):
        part = matmul(kwb[:, r * LANES : (r + 1) * LANES], v_ref[...], 0, 0)
        for rr in range(LANES // R):
            for c in range(nc):
                msend[(r * (LANES // R) + rr) * nc + c] = part[
                    rr * R : (rr + 1) * R, c * LANES : (c + 1) * LANES
                ].astype(bf16)

    pl.semaphore_wait(barrier, NSP - 1 + T - 1)

    mrecv[me] = msend[me]
    st_recv[me] = st_src[...]

    def scatter(p, carry):
        dst = mod(me + p, NSP)
        for src, to, s in ((msend.at[dst], mrecv.at[me], 0), (st_src, st_recv.at[me], 2)):
            pltpu.make_async_remote_copy(
                src_ref=src, dst_ref=to, send_sem=p1.at[s], recv_sem=p1.at[s + 1],
                device_id=at_sp(dst), device_id_type=MESH,
            ).start()
        return carry

    lax.fori_loop(1, NSP, scatter, 0)

    for copy in local:
        copy.wait()

    left, right, across = mod(tp - 1, T), mod(tp + 1, T), mod(tp + 2, T)

    def ring_start(buf, base, half, sems):
        top, bottom = buf.at[ds(base(tp), half)], buf.at[ds(base(tp) + half, half)]
        for k, piece, device in ((0, top, right), (1, bottom, left), (2, bottom, right), (3, top, left)):
            send(piece, piece, sems.at[0, k], sems.at[1, k], at_tp(device))

    def ring_piece(buf, base, half, k):
        block, low = ((left, 0), (right, 1), (left, 1), (right, 0), (across, 0), (across, 1))[k]
        return buf.at[ds(base(block) + low * half, half)]

    def ring_wait(buf, base, half, sems, k):
        piece = ring_piece(buf, base, half, k)
        arrived(piece, sems.at[0, k], sems.at[1, k], at_tp(left))
        if k < 2:
            send(piece, piece, sems.at[0, k + 4], sems.at[1, k + 4], at_tp((right, left)[k]))
        return piece

    wcore = wrows // C
    whalf = wcore // 2

    def wo_base(block):
        return block * wrows + core * wcore

    def wo_twin_base(block):
        return block * wrows + (C - 1 - core) * wcore

    def wo_step(k):
        piece = ring_wait(wo, wo_base, whalf, wos, k)
        if C == 2:
            send(piece, piece, wod.at[0, k], wod.at[1, k], sibling)

    def at_zx(z, x, c):
        return z * (X * C) + x * C + c

    def shard_of(index):
        at = ds(index * shard, shard)
        return (wu.at[at], wd.at[at])

    for w, piece in enumerate(shard_of(me)):
        if C == 2:
            send(piece, piece, xd.at[0, 0, w], xd.at[1, 0, w], sibling)
        for k in range(1, X):
            to = at_sp(at_zx(zz, mod(xx + k, X), core))
            send(piece, piece, xs.at[0, k, w], xs.at[1, k, w], to)
    ring_start(wo, wo_base, whalf, wos)

    def inside(b, carry):
        at = ds(b * ROW_STEP, ROW_STEP)
        here = line + b * ROW_STEP
        logs = jnp.where(lane <= here, runc[at, :] - run_row + li_row, far_below)
        top = jnp.max(logs, axis=1, keepdims=True)
        scores = matmul(q_ref[at, :], k_ref[...], 1, 1) * (jnp.exp(logs - top) * scale)
        m1[at, :] = top
        d1[at, :] = jnp.sum(scores, axis=1, keepdims=True)
        a1[at, :] = matmul(scores.astype(bf16), v_ref[...])
        return carry

    lax.fori_loop(0, steps, inside, 0)

    for k in range(1, X):
        src = at_zx(zz, mod(xx - k, X), core)
        for w, piece in enumerate(shard_of(src)):
            arrived(piece, xs.at[0, k, w], xs.at[1, k, w], at_sp(src))
            if C == 2:
                send(piece, piece, xd.at[0, k, w], xd.at[1, k, w], sibling)

    def all_but_one(buf):
        return buf.at[pl.ds(0, NSP - 1)]

    def bulk(buf, sems, s):
        pltpu.make_async_remote_copy(
            src_ref=all_but_one(buf), dst_ref=all_but_one(buf),
            send_sem=sems.at[s], recv_sem=sems.at[s + 1],
            device_id=at_sp(me), device_id_type=MESH,
        ).wait()

    bulk(mrecv, p1, 0)
    bulk(st_recv, p1, 2)

    def advance(i, state):
        highest, memory, norm = state
        for u in range(8):
            d = i * 8 + u
            ssend[d] = memory.astype(bf16)
            nin[d, 0:nq, :] = norm
            nin[d, nq : nq + 1, :] = highest
            following = st_recv[d]
            decayed = highest + following[nq : nq + 1, :]
            lead_d = following[nq + 1 : nq + 2, :]
            highest = jnp.maximum(decayed, lead_d)
            before = jnp.exp(decayed - highest)
            after = jnp.exp(lead_d - highest)
            memory = before * memory + after * mrecv[d].astype(f32)
            norm = before * norm + after * following[0:nq, :]
        return highest, memory, norm

    lax.fori_loop(
        0, NSP // 8, advance,
        (jnp.full((1, LANES), far_below, f32), jnp.zeros((R, LANES), f32), jnp.zeros((nq, LANES), f32)),
    )
    srecv[me] = ssend[me]

    def give_back(p, carry):
        dst = mod(me + p, NSP)
        pltpu.make_async_remote_copy(
            src_ref=ssend.at[dst], dst_ref=srecv.at[me], send_sem=p2.at[0], recv_sem=p2.at[1],
            device_id=at_sp(dst), device_id_type=MESH,
        ).start()
        return carry

    lax.fori_loop(1, NSP, give_back, 0)

    wo_step(0)
    wo_step(1)

    slab = shard * X * C
    part_rows = slab // C
    half_rows = part_rows // 2
    if C == 2:
        for k in range(X):
            src = at_zx(zz, mod(xx - k, X), 1 - core)
            for w, piece in enumerate(shard_of(src)):
                arrived(piece, xd.at[0, k, w], xd.at[1, k, w], sibling)
    ups = (at_zx(mod(zz + 1, Z), xx, core), at_zx(mod(zz - 1, Z), xx, core))

    def z_piece(w, direction, s, h, c):
        z = mod(zz - s if direction == 0 else zz + s, Z)
        at = ds(z * slab + c * part_rows + h * half_rows, half_rows)
        return (wu, wd)[w].at[at]

    def z_has(direction, s, h):
        return s < Z // 2 or (s == Z // 2 and h == direction)

    def z_send(w, direction, s, h):
        if z_has(direction, s, h):
            piece = z_piece(w, direction, s - 1, h, core)
            i = (s - 1) * 2 + h
            send(
                piece, piece, zs.at[0, direction, w, i], zs.at[1, direction, w, i],
                at_sp(ups[direction]),
            )

    def z_start(w):
        for h in range(2):
            for direction in range(2):
                z_send(w, direction, 1, h)

    def z_step(w, s, h):
        for direction in range(2):
            if z_has(direction, s, h):
                piece = z_piece(w, direction, s, h, core)
                i = (s - 1) * 2 + h
                arrived(
                    piece, zs.at[0, direction, w, i], zs.at[1, direction, w, i],
                    at_sp(ups[direction]),
                )
                z_send(w, direction, s + 1, h)
                if C == 2:
                    send(piece, piece, zd.at[0, direction, w, i], zd.at[1, direction, w, i], sibling)

    def z_twin(w):
        for s in range(1, Z // 2 + 1):
            for h in range(2):
                for direction in range(2):
                    if C == 2 and z_has(direction, s, h):
                        piece = z_piece(w, direction, s, h, 1 - core)
                        i = (s - 1) * 2 + h
                        arrived(piece, zd.at[0, direction, w, i], zd.at[1, direction, w, i], sibling)

    z_events = [(0, s, h) for s in range(1, Z // 2 + 1) for h in range(2)]
    d_events = [(1, s, h) for s in range(1, Z // 2 + 1) for h in range(2)]
    z_start(0)
    for event in z_events[:2]:
        z_step(*event)

    bulk(srecv, p2, 0)
    for j in range(NSP):
        r, c = divmod(j, nc)
        m_in[r * R : (r + 1) * R, c * LANES : (c + 1) * LANES] = srecv[j]
    stats = nin[me]
    normer_in = jnp.concatenate([stats[r : r + 1, :] for r in range(nq)], axis=1)
    stab = stats[nq : nq + 1, 0:1]

    def finish(b, carry):
        at = ds(b * ROW_STEP, ROW_STEP)
        queries = q_ref[at, :]
        carried = runc[at, :] + stab
        top = m1[at, :]
        row_max = jnp.maximum(carried, top)
        inner = jnp.exp(top - row_max)
        outer = jnp.exp(carried - row_max) * scale
        reach = jnp.sum(queries.astype(f32) * normer_in, axis=1, keepdims=True)
        denominator = inner * d1[at, :] + outer * reach
        floor = jnp.maximum(jnp.abs(denominator), jnp.exp(-row_max))
        numerator = inner * a1[at, :] + outer * matmul(queries, m_in[...])
        gate = 1.0 / (1.0 + jnp.exp(-og_ref[at, :].astype(f32)))
        gsend[at, :] = (numerator / floor * gate).astype(bf16)
        return carry

    lax.fori_loop(0, steps, finish, 0)

    grecv[tp] = gsend[ds(tp * own, own), :]
    for k in range(1, T):
        dst = mod(tp + k, T)
        send(gsend.at[ds(dst * own, own)], grecv.at[tp], a2.at[0, k], a2.at[1, k], at_tp(dst))

    wo_step(2)
    wo_step(3)
    for event in z_events[2:4]:
        z_step(*event)
    wo_step(4)
    wo_step(5)
    if C == 2:
        for k in range(6):
            piece = ring_piece(wo, wo_twin_base, whalf, k)
            arrived(piece, wod.at[0, k], wod.at[1, k], sibling)
    for k in range(1, T):
        src = mod(tp - k, T)
        arrived(grecv.at[src], a2.at[0, k], a2.at[1, k], at_tp(src))

    def project(n, carry):
        at = ds(n * TILE, TILE)
        acc = matmul(grecv[0], wo[0:hv, at])
        for h in range(1, T):
            acc = acc + matmul(grecv[h], wo[h * hv : (h + 1) * hv, at])
        mixed[:, at] = acc
        return carry

    lax.fori_loop(0, D // TILE, project, 0)

    def join(b, carry):
        at = ds(b * NORM_STEP, NORM_STEP)
        values = mixed[at, :].astype(bf16).astype(f32)
        joined = (res_ref[at, :].astype(f32) + normalize(values, mixg_ref[...])).astype(bf16)
        stream[at, :] = joined
        rows_all[ds(tp * own + b * NORM_STEP, NORM_STEP), :] = normalize(
            joined.astype(f32), preg_ref[...]
        ).astype(bf16)
        return carry

    lax.fori_loop(0, own // NORM_STEP, join, 0)

    half = own // 2

    def block_base(block):
        return block * own

    ring_start(rows_all, block_base, half, ags)
    for event in z_events[4:6]:
        z_step(*event)
    ring_wait(rows_all, block_base, half, ags, 0)
    ring_wait(rows_all, block_base, half, ags, 1)
    z_start(1)
    for event in z_events[6:]:
        z_step(*event)
    for event in d_events[:2]:
        z_step(*event)
    z_twin(0)
    for k in range(2, 6):
        ring_wait(rows_all, block_base, half, ags, k)

    def raise_tile(n, carry):
        at = ds(n * TILE, TILE)
        upb[8 : 8 + rows, at] = matmul(rows_all[...], wu[:, at]).astype(bf16).astype(f32)
        return carry

    lax.fori_loop(0, 2 * ffd // TILE, raise_tile, 0)

    last = pltpu.make_async_remote_copy(
        src_ref=upb.at[pl.ds(rows, 8)], dst_ref=upb.at[pl.ds(0, 8)],
        send_sem=halo.at[0], recv_sem=halo.at[1],
        device_id=at_sp(mod(me + 1, NSP)), device_id_type=MESH,
    )

    @pl.when(me < NSP - 1)
    def _():
        last.start()

    for event in d_events[2:]:
        z_step(*event)

    @pl.when(me == 0)
    def _():
        upb[0:8, :] = jnp.zeros((8, 2 * ffd), f32)

    @pl.when(me > 0)
    def _():
        last.wait_recv()

    def convolve(b, carry):
        window = ds(b * CONV_STEP, CONV_STEP + 8, CONV_STEP)
        at = ds(b * CONV_STEP, CONV_STEP)
        for c in range(0, ffd, TILE):
            both = []
            for taps, first in ((gk_ref, 0), (vk_ref, ffd)):
                block = upb[window, first + c : first + c + TILE]
                total_taps = 0.0
                for j in range(CONV):
                    low = 8 - CONV + 1 + j
                    total_taps = total_taps + taps[j : j + 1, c : c + TILE] * block[low : low + CONV_STEP]
                both.append(total_taps)
            hidden[at, c : c + TILE] = (both[0] / (1.0 + jnp.exp(-both[0])) * both[1]).astype(bf16)
        return carry

    lax.fori_loop(0, rows // CONV_STEP, convolve, 0)
    z_twin(1)

    def lower(n, carry):
        at = ds(n * TILE, TILE)
        pbuf[:, at] = matmul(hidden[...], wd[at, :], 1, 1).astype(bf16)
        return carry

    lax.fori_loop(0, D // TILE, lower, 0)

    def piece_of(block, low):
        return pbuf.at[ds(block * own + low * half, half)]

    def rs(src, dst, k, device):
        send(src, dst, rss.at[0, k], rss.at[1, k], at_tp(device))

    top, bottom = pl.ds(0, half), pl.ds(half, half)
    rs(piece_of(across, 0), relay_top, 2, right)
    rs(piece_of(across, 1), relay_bot, 3, left)
    rs(piece_of(right, 1), from_left.at[bottom], 0, right)
    rs(piece_of(left, 0), from_right.at[top], 1, left)
    for k, relay, block, low, dst in (
        (2, relay_top, right, 0, from_left.at[top]),
        (3, relay_bot, left, 1, from_right.at[bottom]),
    ):
        arrived(relay, rss.at[0, k], rss.at[1, k], at_tp(left))

        def merge(b, carry, relay=relay, block=block, low=low):
            at = ds(b * NORM_STEP, NORM_STEP)
            there = ds(block * own + low * half + b * NORM_STEP, NORM_STEP)
            relay[at, :] = (relay[at, :].astype(f32) + pbuf[there, :].astype(f32)).astype(bf16)
            return carry

        lax.fori_loop(0, half // NORM_STEP, merge, 0)
        rs(relay, dst, k + 2, (right, left)[k - 2])
    arrived(from_left.at[bottom], rss.at[0, 0], rss.at[1, 0], at_tp(left))
    arrived(from_right.at[top], rss.at[0, 1], rss.at[1, 1], at_tp(right))
    arrived(from_left.at[top], rss.at[0, 4], rss.at[1, 4], at_tp(left))
    arrived(from_right.at[bottom], rss.at[0, 5], rss.at[1, 5], at_tp(right))

    def close(b, carry):
        at = ds(b * NORM_STEP, NORM_STEP)
        summed = (
            pbuf[ds(tp * own + b * NORM_STEP, NORM_STEP), :].astype(f32)
            + from_left[at, :].astype(f32)
            + from_right[at, :].astype(f32)
        )
        values = summed.astype(bf16).astype(f32)
        out_ref[at, :] = (
            stream[at, :].astype(f32) + normalize(values, postg_ref[...])
        ).astype(bf16)
        return carry

    lax.fori_loop(0, own // NORM_STEP, close, 0)

    for copy in pending:
        copy.wait_send()

    @pl.when(me < NSP - 1)
    def _():
        last.wait_send()


def body(
    shape,
    query_rows, key_rows, value_rows, out_gate_pre, input_gate_pre, forget_gate_pre, residual,
    out_proj, mix_gain, pre_gain, gate_proj, value_proj, gate_kernel, value_kernel, down_proj,
    post_gain,
):
    Z, X, C, T = shape
    NSP = Z * X * C
    rows, qk = query_rows.shape
    hv = value_rows.shape[1]
    own, D = residual.shape
    ffd = gate_proj.shape[1]
    R = qk * hv // LANES // NSP
    dma = pltpu.SemaphoreType.DMA
    vm = pltpu.VMEM
    inner = pl.BlockSpec(memory_space=pltpu.VMEM)
    outer = pl.BlockSpec(memory_space=pl.ANY)
    return pl.pallas_call(
        functools.partial(kernel, Z, X, C, T),
        out_shape=jax.ShapeDtypeStruct((own, D), bf16),
        in_specs=[inner] * 12 + [outer] * 4,
        out_specs=inner,
        scratch_shapes=[
            vm((NSP, R, LANES), bf16),
            vm((NSP, R, LANES), bf16),
            vm((4, LANES), f32),
            vm((NSP, 4, LANES), f32),
            vm((NSP, R, LANES), bf16),
            vm((NSP, R, LANES), bf16),
            vm((NSP, 4, LANES), f32),
            vm((qk, hv), bf16),
            vm((rows, qk), bf16),
            vm((rows, 1), f32),
            vm((rows, hv), f32),
            vm((rows, 1), f32),
            vm((rows, 1), f32),
            vm((rows, hv), bf16),
            vm((T, own, hv), bf16),
            vm((T * hv, D), bf16),
            vm((D, 2 * ffd), bf16),
            vm((D, ffd), bf16),
            vm((rows, D), bf16),
            vm((own, D), f32),
            vm((own, D), bf16),
            vm((rows + 8, 2 * ffd), f32),
            vm((rows, ffd), bf16),
            vm((rows, D), bf16),
            vm((own, D), bf16),
            vm((own, D), bf16),
            vm((own // 2, D), bf16),
            vm((own // 2, D), bf16),
            dma((4,)),
            dma((4,)),
            dma((2,)),
            dma((2, X, 2)),
            dma((2, X, 2)),
            dma((2, 2, 2, max(Z, 1))),
            dma((2, 2, 2, max(Z, 1))),
            dma((2, 6)),
            dma((2, 6)),
            dma((2, 6)),
            dma((2, 6)),
            dma((2, T)),
            dma((2,)),
        ],
        compiler_params=pltpu.CompilerParams(
            collective_id=0, has_side_effects=True, vmem_limit_bytes=60 * 1024 * 1024
        ),
        name="cell_and_mixer",
    )(
        query_rows, key_rows, value_rows, out_gate_pre, input_gate_pre, forget_gate_pre, residual,
        mix_gain.reshape(1, D), pre_gain.reshape(1, D), post_gain.reshape(1, D),
        gate_kernel, value_kernel, out_proj, gate_proj, value_proj, down_proj,
    )


def solution(mesh):
    shape = (*SHAPES[mesh.shape["sp"]], mesh.shape["tp"])
    placed = (
        P("sp", "tp"),
        P("sp", "tp"),
        P("sp", "tp"),
        P("sp", "tp"),
        P("tp", "sp"),
        P("tp", "sp"),
        P(("sp", "tp"), None),
        P("tp", None),
        P(),
        P(),
        P("sp", "tp"),
        P("sp", "tp"),
        P(None, "tp"),
        P(None, "tp"),
        P("sp", "tp"),
        P(),
    )
    return jax.shard_map(
        functools.partial(body, shape), mesh=mesh, in_specs=placed,
        out_specs=P(("sp", "tp"), None), check_vma=False,
    )
```

time: 352 us -> 123 us (0.35)
  Pallas kernels: 0 us -> 121 us
  waiting for transfers between devices: 96.4 us -> 0 us
  blocking collectives: 88.3 us -> 0 us
  between operations: 53 us -> 0.01 us
  other arithmetic: 48.6 us -> 0 us
  local copies, waits for them, and re-layouts: 39.1 us -> 1.88 us
  matrix products: 22.7 us -> 0 us
    pallas_call x0 -> x1, Pallas kernels: none -> 121 us  [body(): pl.pallas_call(functools.partial(kernel, Z, X, C, T), out_shape=jax.Shape...]
    all_gather x4 -> x0, waiting for transfers between devices: 93.7 us -> none  [the longest x3 93.7 us: all_in_one(): both, at, found = (lax.all_gather(jnp.concatenate(lines), axis), 0, {})]
    all_to_all x3 -> x0, blocking collectives: 88.3 us -> none  [the longest x2 59.7 us: sum_at_owner(): lax.all_to_all(blocks, axis, split_axis=0, concat_axis=0, tiled=True)]
    dot_general x9 -> x0, matrix products: 22.7 us -> none  [the longest x1 4.59 us: body(): lax.dot_general(rows_part, full_down, (((1,), (1,)), ((), ())), preferred...]
    add x25 -> x0, other arithmetic: 18.9 us -> none  [the longest x13 11.4 us: body(): inclusive = lax.associative_scan(combine, segments, axis=1)]
    slice x39 -> x0, local copies, waits for them, and re-layouts: 16.4 us -> none  [the longest x2 5.64 us: body(): member[:, :-1]]
    pad x24 -> x0, local copies, waits for them, and re-layouts: 13.6 us -> none  [the longest x15 12.2 us: body(): inclusive = lax.associative_scan(combine, segments, axis=1)]
    mul x9 -> x0, other arithmetic: 6.18 us -> none  [the longest x4 4.08 us: combine(): prev_scale[..., None, None] * prev_memory]
  transfers between devices with their start and end apart: 5 -> 0, of which waited for: 4 -> 0; matrix products, arithmetic and copies ran while one was open for 8% -> 0% of each run, Pallas kernels for 0% -> 0%
where the time goes in v1:
time: 123 us
  Pallas kernels  121 us (98%)
  local copies, waits for them, and re-layouts  1.88 us (2%)
    pallas_call x1, Pallas kernels, body(): pl.pallas_call(functools.partial(kernel, Z, X, C, T), out_shape=jax.Shape...  121 us

profile of v1, /device:TPU:2, one launch (start us, length us, event | category | flops | bytes accessed | tf_op | source)
XLA Modules:
  0.0 122.8 jit_solution(17941173331795182786)
XLA Ops:
  0.0 120.9 %cell_and_mixer.1 = bf16[128,2048]{1,0:T(8,128)(2,1)} custom-call(bf16[512,256]{1,0:T(8,128)(2,1)} %q_ref.1, bf16[512,256]{1,0:T(8,128)(2,1)} %k_ref.1, bf16[512,512]{1,0:T(8,128)(2,1)} %v_ref.1, bf16[512,512]{1,0:T(8,128)(2,1)} %og_ref.1, f32[1,512]{1,0:T(1,128)} %ig_ref.1, f32[1,512]{1,0:T(1,128)} %fg_ref.1, bf16[128,2048]{1,0:T(8,128)(2,1)} %res_ref.1, ...), custom_call_target="tpu_custom_call" | custom-call | tf_op jit(solution)/shard_map/cell_and_mixer/pallas_call | solution.py:574
  121.0 1.9 %copy.18 = bf16[128,2048]{1,0:T(8,128)(2,1)} copy(bf16[128,2048]{1,0:T(8,128)(2,1)} %cell_and_mixer.1) | data formatting | bytes 1048576

commit v2 on v1

v2 whole, which is shorter than its diff:
```python
import functools

import jax
import jax.numpy as jnp
from jax import lax
from jax.experimental import pallas as pl
from jax.experimental.pallas import tpu as pltpu
from jax.sharding import PartitionSpec as P

f32 = jnp.float32
bf16 = jnp.bfloat16
MESH = pl.DeviceIdType.MESH

gate_cap = 15.0
epsilon = 1e-06
far_below = -1e30
CONV = 3
LANES = 128
ROW_STEP = 64
NORM_STEP = 16
CONV_STEP = 32
TILE = 256
HALO = 16

SHAPES = {64: (8, 4, 2)}


def softcap(values):
    return gate_cap * jnp.tanh(values * (1.0 / gate_cap))


def log_one_plus(values):
    series = values * (
        1.0 + values * (-1 / 2 + values * (1 / 3 + values * (-1 / 4 + values * (1 / 5))))
    )
    return jnp.where(values < 0.015625, series, jnp.log(1.0 + values))


def log_sigmoid(values):
    return jnp.minimum(values, 0.0) - log_one_plus(jnp.exp(-jnp.abs(values)))


def normalize(values, gains):
    return values * lax.rsqrt(jnp.mean(values * values, axis=-1, keepdims=True) + epsilon) * gains


def matmul(left, right, left_dim=1, right_dim=0):
    return lax.dot_general(
        left, right, (((left_dim,), (right_dim,)), ((), ())), preferred_element_type=f32
    )


def mod(value, size):
    return lax.rem(value + size, jnp.int32(size))


def kernel(
    Z, X, C, T,
    q_in, k_in, v_in, og_in, ig_in, fg_in, res_in, mixg_in, preg_in, postg_in, gk_in, vk_in,
    outp_ref, gatep_ref, valuep_ref, downp_ref,
    out_ref,
    q_ref, k_ref, v_ref, og_ref, ig_ref, fg_ref, res_ref, mixg_ref, preg_ref, postg_ref, gk_own, vk_own,
    msend, mrecv, st_src, st_recv, ssend, srecv, nin, m_in, kwb, runc, a1, m1, d1,
    gated, wo, ushard, wu, dshard, wd, gk_ref, vk_ref, rows_all, stream, upb, hidden,
    mix_part, mix_left, mix_right, mix_top, mix_bot,
    ffn_part, ffn_left, ffn_right, ffn_top, ffn_bot,
    loc, loaded, p1, p2, xs, xd, zs, zd, taps, ags, mss, rss, halo,
):
    NSP = Z * X * C
    rows, qk = q_ref.shape
    hv = v_ref.shape[1]
    own, D = out_ref.shape
    ffd = gatep_ref.shape[1]
    scale = float(qk) ** -0.5
    me = lax.axis_index("sp")
    tp = lax.axis_index("tp")
    core = lax.rem(me, jnp.int32(C))
    xx = lax.rem(lax.div(me, jnp.int32(C)), jnp.int32(X))
    zz = lax.div(me, jnp.int32(C * X))
    pending = []

    def at_sp(index):
        return {"sp": index, "tp": tp}

    def at_tp(index):
        return {"sp": me, "tp": index}

    def at_zx(z, x, c):
        return z * (X * C) + x * C + c

    def remote(src, dst, ssem, rsem, device):
        return pltpu.make_async_remote_copy(
            src_ref=src, dst_ref=dst, send_sem=ssem, recv_sem=rsem,
            device_id=device, device_id_type=MESH,
        )

    def send(src, dst, ssem, rsem, device):
        copy = remote(src, dst, ssem, rsem, device)
        copy.start()
        pending.append(copy)

    def send_if(condition, src, dst, ssem, rsem, device):
        copy = remote(src, dst, ssem, rsem, device)
        pl.when(condition)(copy.start)
        pending.append((condition, copy))

    def arrived(dst, ssem, rsem, device):
        remote(dst, dst, ssem, rsem, device).wait_recv()

    def ds(start, size, step=None):
        return pl.ds(pl.multiple_of(start, step or size), size)

    sibling = at_sp(me + 1 - 2 * core)

    units = lax.rem(xx + tp, jnp.int32(T))

    def holder(x):
        return {"sp": at_zx(zz, x, core), "tp": mod(tp - x, T)}

    def source(x):
        return {"sp": at_zx(zz, x, core), "tp": units}

    barrier = pltpu.get_barrier_semaphore()

    def greet(p, carry):
        pl.semaphore_signal(
            barrier, 1, device_id=at_sp(mod(me + p, NSP)), device_id_type=MESH
        )
        return carry

    lax.fori_loop(1, NSP, greet, 0)
    for k in range(1, T):
        pl.semaphore_signal(barrier, 1, device_id=at_tp(mod(tp + k, T)), device_id_type=MESH)
    for k in range(X):

        @pl.when(xx + k > 0)
        def _(k=k):
            pl.semaphore_signal(barrier, 1, device_id=source(k), device_id_type=MESH)

    loads = [
        pltpu.make_async_copy(src, dst, loaded.at[i])
        for i, (src, dst) in enumerate((
            (ig_in, ig_ref), (fg_in, fg_ref), (k_in, k_ref), (v_in, v_ref), (q_in, q_ref),
            (og_in, og_ref), (res_in, res_ref), (mixg_in, mixg_ref), (preg_in, preg_ref),
            (postg_in, postg_ref), (gk_in, gk_own), (vk_in, vk_own),
        ))
    ]
    shard = gatep_ref.shape[0]
    local = [
        pltpu.make_async_copy(gatep_ref, ushard.at[:, pl.ds(0, ffd)], loc.at[0]),
        pltpu.make_async_copy(valuep_ref, ushard.at[:, pl.ds(ffd, ffd)], loc.at[1]),
        pltpu.make_async_copy(downp_ref, dshard, loc.at[2]),
        pltpu.make_async_copy(outp_ref, wo, loc.at[3]),
    ]
    for copy in loads + local:
        copy.start()

    steps = rows // ROW_STEP
    lane = lax.broadcasted_iota(jnp.int32, (ROW_STEP, rows), 1)
    line = lax.broadcasted_iota(jnp.int32, (ROW_STEP, rows), 0)
    loads[0].wait()
    loads[1].wait()
    li_row = softcap(ig_ref[...])
    lf_row = log_sigmoid(softcap(fg_ref[...]))

    def sums(b, run_row):
        here = line + b * ROW_STEP
        run_col = jnp.sum(jnp.where(lane <= here, lf_row, 0.0), axis=1, keepdims=True)
        runc[ds(b * ROW_STEP, ROW_STEP), :] = run_col
        return run_row + jnp.sum(jnp.where(lane == here, run_col, 0.0), axis=0, keepdims=True)

    run_row = lax.fori_loop(0, steps, sums, jnp.zeros((1, rows), f32))
    total = run_row[:, rows - 1 : rows]
    lead = total - run_row + li_row
    lead_max = jnp.max(lead, axis=1, keepdims=True)
    lead_weights = jnp.exp(lead - lead_max)
    loads[2].wait()
    loads[3].wait()

    def weigh(b, normer):
        here = line + b * ROW_STEP
        at = ds(b * ROW_STEP, ROW_STEP)
        column = jnp.sum(jnp.where(lane == here, lead_weights, 0.0), axis=1, keepdims=True)
        weighted = k_ref[at, :].astype(f32) * column
        kwb[at, :] = weighted.astype(bf16)
        return normer + jnp.sum(weighted, axis=0, keepdims=True)

    normer = lax.fori_loop(0, steps, weigh, jnp.zeros((1, qk), f32))
    nq = qk // LANES
    for r in range(nq):
        st_src[r : r + 1, :] = normer[:, r * LANES : (r + 1) * LANES]
    for r in range(nq, 4):
        st_src[r : r + 1, :] = jnp.broadcast_to(total if r == nq else lead_max, (1, LANES))
    R = msend.shape[1]
    nc = hv // LANES
    for r in range(nq):
        part = matmul(kwb[:, r * LANES : (r + 1) * LANES], v_ref[...], 0, 0)
        for rr in range(LANES // R):
            for c in range(nc):
                msend[(r * (LANES // R) + rr) * nc + c] = part[
                    rr * R : (rr + 1) * R, c * LANES : (c + 1) * LANES
                ].astype(bf16)

    with jax.named_scope("barrier"):
        pl.semaphore_wait(barrier, NSP - 1 + T - 1 + X - 1 + jnp.minimum(xx, 1))

    mrecv[me] = msend[me]
    st_recv[me] = st_src[...]

    def scatter(p, carry):
        dst = mod(me + p, NSP)
        remote(msend.at[dst], mrecv.at[me], p1.at[0], p1.at[1], at_sp(dst)).start()
        remote(st_src, st_recv.at[me], p1.at[2], p1.at[3], at_sp(dst)).start()
        return carry

    with jax.named_scope("scatter"):
        lax.fori_loop(1, NSP, scatter, 0)

    left, right, across = mod(tp - 1, T), mod(tp + 1, T), mod(tp + 2, T)
    along_y = (tp, left, right, across, at_tp)

    def ring_start(buf, base, half, sems, ring):
        me_r, left_r, right_r, across_r, at = ring
        top, bottom = buf.at[ds(base(me_r), half, 16)], buf.at[ds(base(me_r) + half, half, 16)]
        for k, piece, device in ((0, top, right_r), (1, bottom, left_r), (2, bottom, right_r), (3, top, left_r)):
            send(piece, piece, sems.at[0, k], sems.at[1, k], at(device))

    def ring_piece(buf, base, half, ring, k):
        me_r, left_r, right_r, across_r, at = ring
        block, low = (
            (left_r, 0), (right_r, 1), (left_r, 1), (right_r, 0), (across_r, 0), (across_r, 1)
        )[k]
        return buf.at[ds(base(block) + low * half, half, 16)]

    def ring_wait(buf, base, half, sems, ring, k):
        piece = ring_piece(buf, base, half, ring, k)
        arrived(piece, sems.at[0, k], sems.at[1, k], ring[4](ring[1]))
        if k < 2:
            to = ring[4]((ring[2], ring[1])[k])
            send(piece, piece, sems.at[0, k + 4], sems.at[1, k + 4], to)
        return piece

    for copy in local:
        copy.wait()
    for copy in loads[4:]:
        copy.wait()

    def rows_of(index):
        return ds(index * shard, shard)

    weights = ((ushard, wu), (dshard, wd))
    for w, (src, dst) in enumerate(weights):
        for k in range(X):
            send_if(
                xx + k > 0, src, dst.at[rows_of(me)], xs.at[0, k, w], xs.at[1, xx, w], holder(k)
            )

    @pl.when(xx == 0)
    def _():
        for src, dst in weights:
            dst[rows_of(me), :] = src[...]

    for i, (src, dst) in enumerate(((gk_own, gk_ref), (vk_own, vk_ref))):
        send_if(xx > 0, src, dst, taps.at[0, i], taps.at[1, i], at_tp(mod(tp - xx, T)))

    @pl.when(xx == 0)
    def _():
        gk_ref[...] = gk_own[...]
        vk_ref[...] = vk_own[...]

    def inside(b, carry):
        at = ds(b * ROW_STEP, ROW_STEP)
        here = line + b * ROW_STEP
        logs = jnp.where(lane <= here, runc[at, :] - run_row + li_row, far_below)
        top = jnp.max(logs, axis=1, keepdims=True)
        scores = matmul(q_ref[at, :], k_ref[...], 1, 1) * (jnp.exp(logs - top) * scale)
        m1[at, :] = top
        d1[at, :] = jnp.sum(scores, axis=1, keepdims=True)
        a1[at, :] = matmul(scores.astype(bf16), v_ref[...])
        return carry

    with jax.named_scope("inside"):
        lax.fori_loop(0, steps, inside, 0)

    def shards(w):
        for k in range(X):
            piece = weights[w][1].at[rows_of(at_zx(zz, k, core))]

            @pl.when(xx + k > 0)
            def _():
                arrived(piece, xs.at[0, k, w], xs.at[1, k, w], source(k))

            send(piece, piece, xd.at[0, k, w], xd.at[1, k, w], sibling)

    def shard_twins(w):
        for k in range(X):
            piece = weights[w][1].at[rows_of(at_zx(zz, k, 1 - core))]
            arrived(piece, xd.at[0, k, w], xd.at[1, k, w], sibling)

    with jax.named_scope("ushards"):
        shards(0)

    def all_but_one(buf):
        return buf.at[pl.ds(0, NSP - 1)]

    def bulk(buf, sems, s):
        remote(all_but_one(buf), all_but_one(buf), sems.at[s], sems.at[s + 1], at_sp(me)).wait()

    with jax.named_scope("p1wait"):
        bulk(mrecv, p1, 0)
        bulk(st_recv, p1, 2)

    def advance(i, state):
        highest, memory, norm = state
        for u in range(8):
            d = i * 8 + u
            ssend[d] = memory.astype(bf16)
            nin[d, 0:nq, :] = norm
            nin[d, nq : nq + 1, :] = highest
            following = st_recv[d]
            decayed = highest + following[nq : nq + 1, :]
            lead_d = following[nq + 1 : nq + 2, :]
            highest = jnp.maximum(decayed, lead_d)
            before = jnp.exp(decayed - highest)
            after = jnp.exp(lead_d - highest)
            memory = before * memory + after * mrecv[d].astype(f32)
            norm = before * norm + after * following[0:nq, :]
        return highest, memory, norm

    lax.fori_loop(
        0, NSP // 8, advance,
        (jnp.full((1, LANES), far_below, f32), jnp.zeros((R, LANES), f32), jnp.zeros((nq, LANES), f32)),
    )
    srecv[me] = ssend[me]

    def give_back(p, carry):
        dst = mod(me + p, NSP)
        remote(ssend.at[dst], srecv.at[me], p2.at[0], p2.at[1], at_sp(dst)).start()
        return carry

    with jax.named_scope("giveback"):
        lax.fori_loop(1, NSP, give_back, 0)

    slab = shard * X * C
    part_rows = slab // C
    half_rows = part_rows // 2
    ups = (at_zx(mod(zz + 1, Z), xx, core), at_zx(mod(zz - 1, Z), xx, core))

    def z_piece(w, direction, s, h, c):
        z = mod(zz - s if direction == 0 else zz + s, Z)
        return weights[w][1].at[ds(z * slab + c * part_rows + h * half_rows, half_rows)]

    def z_has(direction, s, h):
        return s < Z // 2 or (s == Z // 2 and h == direction)

    def z_send(w, direction, s, h):
        if z_has(direction, s, h):
            piece = z_piece(w, direction, s - 1, h, core)
            i = (s - 1) * 2 + h
            send(
                piece, piece, zs.at[0, w, direction, i], zs.at[1, w, direction, i],
                at_sp(ups[direction]),
            )

    def z_start(w):
        for h in range(2):
            for direction in range(2):
                z_send(w, direction, 1, h)

    def z_step(w, s, h):
        with jax.named_scope(("uring", "dring")[w] + str(s) + str(h)):
            for direction in range(2):
                if z_has(direction, s, h):
                    piece = z_piece(w, direction, s, h, core)
                    i = (s - 1) * 2 + h
                    arrived(
                        piece, zs.at[0, w, direction, i], zs.at[1, w, direction, i],
                        at_sp(ups[direction]),
                    )
                    z_send(w, direction, s + 1, h)
                    send(piece, piece, zd.at[0, w, direction, i], zd.at[1, w, direction, i], sibling)

    def z_twin(w):
        with jax.named_scope(("utwin", "dtwin")[w]):
            for s in range(1, Z // 2 + 1):
                for h in range(2):
                    for direction in range(2):
                        if z_has(direction, s, h):
                            piece = z_piece(w, direction, s, h, 1 - core)
                            i = (s - 1) * 2 + h
                            arrived(
                                piece, zd.at[0, w, direction, i], zd.at[1, w, direction, i], sibling
                            )

    u_events = [(0, s, h) for s in range(1, Z // 2 + 1) for h in range(2)]
    d_events = [(1, s, h) for s in range(1, Z // 2 + 1) for h in range(2)]

    def z_next(events):
        if events:
            z_step(*events.pop(0))

    with jax.named_scope("ushtwins"):
        shard_twins(0)
    z_start(0)
    z_next(u_events)

    with jax.named_scope("p2wait"):
        bulk(srecv, p2, 0)
    for j in range(NSP):
        r, c = divmod(j, nc)
        m_in[r * R : (r + 1) * R, c * LANES : (c + 1) * LANES] = srecv[j]
    stats = nin[me]
    normer_in = jnp.concatenate([stats[r : r + 1, :] for r in range(nq)], axis=1)
    stab = stats[nq : nq + 1, 0:1]

    def finish(b, carry):
        at = ds(b * ROW_STEP, ROW_STEP)
        queries = q_ref[at, :]
        carried = runc[at, :] + stab
        top = m1[at, :]
        row_max = jnp.maximum(carried, top)
        inner = jnp.exp(top - row_max)
        outer = jnp.exp(carried - row_max) * scale
        reach = jnp.sum(queries.astype(f32) * normer_in, axis=1, keepdims=True)
        denominator = inner * d1[at, :] + outer * reach
        floor = jnp.maximum(jnp.abs(denominator), jnp.exp(-row_max))
        numerator = inner * a1[at, :] + outer * matmul(queries, m_in[...])
        gate = 1.0 / (1.0 + jnp.exp(-og_ref[at, :].astype(f32)))
        gated[at, :] = (numerator / floor * gate).astype(bf16)
        return carry

    with jax.named_scope("finish"):
        lax.fori_loop(0, steps, finish, 0)

    half = own // 2
    top, bottom = pl.ds(0, half), pl.ds(half, half)

    class Sums:
        def __init__(self, piece, ring, sems, from_left, from_right, relay_top, relay_bot):
            self.piece, self.ring, self.sems = piece, ring, sems
            self.from_left, self.from_right = from_left, from_right
            self.relays = (relay_top, relay_bot)

        def send(self, src, dst, k, side):
            to = self.ring[4](self.ring[side])
            send(src, dst, self.sems.at[0, k], self.sems.at[1, k], to)

        def wait(self, dst, k):
            arrived(dst, self.sems.at[0, k], self.sems.at[1, k], self.ring[4](self.ring[1]))

        def far(self):
            self.send(self.piece(3, 0, half)[0], self.relays[0], 2, 2)
            self.send(self.piece(3, 1, half)[0], self.relays[1], 3, 1)

        def near(self):
            self.send(self.piece(2, 1, half)[0], self.from_left.at[bottom], 0, 2)
            self.send(self.piece(1, 0, half)[0], self.from_right.at[top], 1, 1)

        def relay(self):
            for k, relay, side, low, dst in (
                (2, self.relays[0], 2, 0, self.from_left.at[top]),
                (3, self.relays[1], 1, 1, self.from_right.at[bottom]),
            ):
                with jax.named_scope("relay"):
                    self.wait(relay, k)
                own_piece = self.piece(side, low, half)[0]

                def merge(b, carry, relay=relay, own_piece=own_piece):
                    at = ds(b * NORM_STEP, NORM_STEP)
                    relay[at, :] = (relay[at, :].astype(f32) + own_piece[at, :].astype(f32)).astype(bf16)
                    return carry

                lax.fori_loop(0, half // NORM_STEP, merge, 0)
                self.send(relay, dst, k + 2, side)

        def finish(self):
            with jax.named_scope("sumwait"):
                self.wait(self.from_left.at[bottom], 0)
                self.wait(self.from_right.at[top], 1)
                self.wait(self.from_left.at[top], 4)
                self.wait(self.from_right.at[bottom], 5)

        def total(self, b):
            at = ds(b * NORM_STEP, NORM_STEP)
            mine = self.piece(0, 0, own)[0]
            summed = (
                mine[at, :].astype(f32)
                + self.from_left[at, :].astype(f32)
                + self.from_right[at, :].astype(f32)
            )
            return summed.astype(bf16).astype(f32)

    def mix_piece(side, low, size):
        return (mix_part.at[ds(along_y[side] * own + low * half, size, half)],)

    mixes = Sums(mix_piece, along_y, mss, mix_left, mix_right, mix_top, mix_bot)

    def project(n, carry):
        at = ds(n * TILE, TILE)
        mix_part[:, at] = matmul(gated[...], wo[:, at]).astype(bf16)
        return carry

    with jax.named_scope("project"):
        lax.fori_loop(0, D // TILE, project, 0)
    mixes.far()
    mixes.near()
    z_next(u_events)
    z_next(u_events)
    mixes.relay()
    z_next(u_events)
    with jax.named_scope("dshards"):
        shards(1)
    z_next(u_events)
    with jax.named_scope("dshtwins"):
        shard_twins(1)
    z_start(1)
    mixes.finish()
    z_next(u_events)

    def at_ring(index):
        return {
            "sp": me + core * (at_zx(zz, index, core) - me),
            "tp": index + core * (tp - index),
        }

    spot = tp + core * (xx - tp)
    fl, fr, fo = mod(spot - 1, T), mod(spot + 1, T), mod(spot + 2, T)
    ring = (spot, fl, fr, fo, at_ring)
    block_rows = own + HALO

    def block_base(block):
        return block * block_rows + HALO

    def join(b, carry):
        at = ds(b * NORM_STEP, NORM_STEP)
        values = mixes.total(b)
        joined = (res_ref[at, :].astype(f32) + normalize(values, mixg_ref[...])).astype(bf16)
        stream[at, :] = joined
        rows_all[ds(block_base(spot) + b * NORM_STEP, NORM_STEP), :] = normalize(
            joined.astype(f32), preg_ref[...]
        ).astype(bf16)
        return carry

    with jax.named_scope("join"):
        lax.fori_loop(0, own // NORM_STEP, join, 0)

    ring_start(rows_all, block_base, half, ags, ring)

    place = me * T + tp
    after = place + 1
    is_last = after == NSP * T
    nsp = lax.rem(lax.div(after, jnp.int32(T)), jnp.int32(NSP))
    ntp = lax.rem(after, jnp.int32(T))
    ncore = lax.rem(nsp, jnp.int32(C))
    nx = lax.rem(lax.div(nsp, jnp.int32(C)), jnp.int32(X))
    nz = lax.div(nsp, jnp.int32(C * X))
    slot = ntp + ncore * (nx - ntp)
    tail = rows_all.at[ds(block_base(spot) + own - HALO, HALO, 16)]
    tail_to = rows_all.at[ds(slot * block_rows, HALO, 16)]
    for k in range(T):
        to_sp = nsp + ncore * (at_zx(nz, k, ncore) - nsp)
        to_tp = k + ncore * (ntp - k)
        to_self = to_sp * T + to_tp == place
        go = jnp.logical_not(jnp.logical_or(is_last, to_self))
        send_if(go, tail, tail_to, halo.at[0, k], halo.at[1, slot], {"sp": to_sp, "tp": to_tp})

        @pl.when(jnp.logical_and(to_self, jnp.logical_not(is_last)))
        def _():
            rows_all[ds(slot * block_rows, HALO, 16), :] = rows_all[
                ds(block_base(spot) + own - HALO, HALO, 16), :
            ]

    def halo_wait(block):
        device = at_ring(block)
        ahead = device["sp"] * T + device["tp"] - 1
        here = rows_all.at[ds(block * block_rows, HALO, 16)]

        @pl.when(ahead < 0)
        def _():
            rows_all[ds(block * block_rows, HALO, 16), :] = jnp.zeros((HALO, D), bf16)

        @pl.when(jnp.logical_and(ahead >= 0, ahead != place))
        def _():
            arrived(here, halo.at[0, 0], halo.at[1, block], device)

    def ag_wait(k):
        with jax.named_scope("ag" + str(k)):
            ring_wait(rows_all, block_base, half, ags, ring, k)

    while u_events:
        z_next(u_events)
    z_next(d_events)
    ag_wait(0)
    ag_wait(1)

    @pl.when(xx > 0)
    def _():
        for i, dst in enumerate((gk_ref, vk_ref)):
            arrived(dst, taps.at[0, i], taps.at[1, i], at_tp(mod(tp + xx, T)))

    z_twin(0)

    def mix(block, place_in):
        halo_wait(block)
        lines = ds(block * block_rows, block_rows, 16)

        def raise_tile(n, carry):
            at = ds(n * TILE, TILE)
            upb[:, at] = matmul(rows_all[lines, :], wu[:, at]).astype(bf16).astype(f32)
            return carry

        with jax.named_scope("raise"):
            lax.fori_loop(0, 2 * ffd // TILE, raise_tile, 0)

        def convolve(b, carry):
            window = ds(b * CONV_STEP + HALO - 8, CONV_STEP + 8, 8)
            at = ds(b * CONV_STEP + place_in * own, CONV_STEP)
            for c in range(0, ffd, TILE):
                both = []
                for taps_ref, first in ((gk_ref, 0), (vk_ref, ffd)):
                    block_values = upb[window, first + c : first + c + TILE]
                    summed = 0.0
                    for j in range(CONV):
                        low = 8 - CONV + 1 + j
                        summed = summed + taps_ref[j : j + 1, c : c + TILE] * block_values[low : low + CONV_STEP]
                    both.append(summed)
                hidden[at, c : c + TILE] = (both[0] / (1.0 + jnp.exp(-both[0])) * both[1]).astype(bf16)
            return carry

        with jax.named_scope("conv"):
            lax.fori_loop(0, own // CONV_STEP, convolve, 0)

    order = (3, 2, 1, 0)

    def lower(first, last):
        lines = pl.ds(first * own, (last - first) * own)

        def lower_tile(n, carry):
            at = ds(n * TILE, TILE)
            ffn_part[lines, at] = matmul(hidden[lines, :], wd[at, :], 1, 1).astype(bf16)
            return carry

        with jax.named_scope("lower"):
            lax.fori_loop(0, D // TILE, lower_tile, 0)

    def ffn_piece(side, low, size):
        return (ffn_part.at[pl.ds(order.index(side) * own + low * half, size)],)

    ffns = Sums(ffn_piece, ring, rss, ffn_left, ffn_right, ffn_top, ffn_bot)
    mix(spot, 3)
    z_next(d_events)
    ag_wait(2)
    mix(fl, 2)
    z_next(d_events)
    ag_wait(3)
    mix(fr, 1)
    z_next(d_events)
    ag_wait(4)
    ag_wait(5)
    mix(fo, 0)
    while d_events:
        z_next(d_events)
    z_twin(1)
    lower(0, 1)
    ffns.far()
    lower(1, T)
    ffns.near()
    ffns.relay()
    ffns.finish()

    def close(b, carry):
        at = ds(b * NORM_STEP, NORM_STEP)
        values = ffns.total(b)
        out_ref[at, :] = (
            stream[at, :].astype(f32) + normalize(values, postg_ref[...])
        ).astype(bf16)
        return carry

    with jax.named_scope("close"):
        lax.fori_loop(0, own // NORM_STEP, close, 0)

    for copy in pending:
        if isinstance(copy, tuple):
            pl.when(copy[0])(copy[1].wait_send)
        else:
            copy.wait_send()


def body(
    shape,
    query_rows, key_rows, value_rows, out_gate_pre, input_gate_pre, forget_gate_pre, residual,
    out_proj, mix_gain, pre_gain, gate_proj, value_proj, gate_kernel, value_kernel, down_proj,
    post_gain,
):
    Z, X, C, T = shape
    NSP = Z * X * C
    rows, qk = query_rows.shape
    hv = value_rows.shape[1]
    own, D = residual.shape
    ffd = gate_proj.shape[1]
    R = qk * hv // LANES // NSP
    dma = pltpu.SemaphoreType.DMA
    vm = pltpu.VMEM
    inner = pl.BlockSpec(memory_space=pltpu.VMEM)
    outer = pl.BlockSpec(memory_space=pl.ANY)
    return pl.pallas_call(
        functools.partial(kernel, Z, X, C, T),
        out_shape=jax.ShapeDtypeStruct((own, D), bf16),
        in_specs=[outer] * 16,
        out_specs=inner,
        scratch_shapes=[
            vm((rows, qk), bf16),
            vm((rows, qk), bf16),
            vm((rows, hv), bf16),
            vm((rows, hv), bf16),
            vm((1, rows), f32),
            vm((1, rows), f32),
            vm((own, D), bf16),
            vm((1, D), f32),
            vm((1, D), f32),
            vm((1, D), f32),
            vm((CONV, ffd), f32),
            vm((CONV, ffd), f32),
            vm((NSP, R, LANES), bf16),
            vm((NSP, R, LANES), bf16),
            vm((4, LANES), f32),
            vm((NSP, 4, LANES), f32),
            vm((NSP, R, LANES), bf16),
            vm((NSP, R, LANES), bf16),
            vm((NSP, 4, LANES), f32),
            vm((qk, hv), bf16),
            vm((rows, qk), bf16),
            vm((rows, 1), f32),
            vm((rows, hv), f32),
            vm((rows, 1), f32),
            vm((rows, 1), f32),
            vm((rows, hv), bf16),
            vm((hv, D), bf16),
            vm((D // NSP, 2 * ffd), bf16),
            vm((D, 2 * ffd), bf16),
            vm((D // NSP, ffd), bf16),
            vm((D, ffd), bf16),
            vm((CONV, ffd), f32),
            vm((CONV, ffd), f32),
            vm((T * (own + HALO), D), bf16),
            vm((own, D), bf16),
            vm((own + HALO, 2 * ffd), f32),
            vm((rows, ffd), bf16),
        ]
        + 2 * [
            vm((rows, D), bf16),
            vm((own, D), bf16),
            vm((own, D), bf16),
            vm((own // 2, D), bf16),
            vm((own // 2, D), bf16),
        ]
        + [
            dma((4,)),
            dma((12,)),
            dma((4,)),
            dma((2,)),
            dma((2, X, 2)),
            dma((2, X, 2)),
            dma((2, 2, 2, Z)),
            dma((2, 2, 2, Z)),
            dma((2, 2)),
            dma((2, 6)),
            dma((2, 6)),
            dma((2, 6)),
            dma((2, T)),
        ],
        compiler_params=pltpu.CompilerParams(
            collective_id=0, has_side_effects=True, vmem_limit_bytes=60 * 1024 * 1024
        ),
        name="cell_and_mixer",
    )(
        query_rows, key_rows, value_rows, out_gate_pre, input_gate_pre, forget_gate_pre, residual,
        mix_gain.reshape(1, D), pre_gain.reshape(1, D), post_gain.reshape(1, D),
        gate_kernel, value_kernel, out_proj, gate_proj, value_proj, down_proj,
    )


def solution(mesh):
    shape = (*SHAPES[mesh.shape["sp"]], mesh.shape["tp"])
    placed = (
        P("sp", "tp"),
        P("sp", "tp"),
        P("sp", "tp"),
        P("sp", "tp"),
        P("tp", "sp"),
        P("tp", "sp"),
        P(("sp", "tp"), None),
        P("tp", None),
        P(),
        P(),
        P("sp", "tp"),
        P("sp", "tp"),
        P(None, "tp"),
        P(None, "tp"),
        P("sp", "tp"),
        P(),
    )
    return jax.shard_map(
        functools.partial(body, shape), mesh=mesh, in_specs=placed,
        out_specs=P(("sp", "tp"), None), check_vma=False,
    )
```

time: 123 us -> 109 us (0.89)
  Pallas kernels: 121 us -> 107 us
    pallas_call x1, Pallas kernels: 121 us -> 107 us  [body(): pl.pallas_call(functools.partial(kernel, Z, X, C, T), out_shape=jax.Shape...]
where the time goes in v2:
time: 109 us
  Pallas kernels  107 us (98%)
  local copies, waits for them, and re-layouts  1.88 us (2%)
    pallas_call x1, Pallas kernels, body(): pl.pallas_call(functools.partial(kernel, Z, X, C, T), out_shape=jax.Shape...  107 us

profile of v2, /device:TPU:2, one launch (start us, length us, event | category | flops | bytes accessed | tf_op | source)
XLA Modules:
  0.0 108.6 jit_solution(3657830076253479386)
XLA Ops:
  0.0 106.7 %cell_and_mixer.1 = bf16[128,2048]{1,0:T(8,128)(2,1)} custom-call(bf16[512,256]{1,0:T(8,128)(2,1)} %q_in.1, bf16[512,256]{1,0:T(8,128)(2,1)} %k_in.1, bf16[512,512]{1,0:T(8,128)(2,1)} %v_in.1, bf16[512,512]{1,0:T(8,128)(2,1)} %og_in.1, f32[1,512]{1,0:T(1,128)} %ig_in.1, f32[1,512]{1,0:T(1,128)} %fg_in.1, bf16[128,2048]{1,0:T(8,128)(2,1)} %res_in.1, ...), custom_call_target="tpu_custom_call" | custom-call | tf_op jit(solution)/shard_map/cell_and_mixer/pallas_call | solution.py:706
  106.7 1.9 %copy.18 = bf16[128,2048]{1,0:T(8,128)(2,1)} copy(bf16[128,2048]{1,0:T(8,128)(2,1)} %cell_and_mixer.1) | data formatting | bytes 1048576

commit v3 on v2

v3 whole, which is shorter than its diff:
```python
import functools

import jax
import jax.numpy as jnp
from jax import lax
from jax.experimental import pallas as pl
from jax.experimental.pallas import tpu as pltpu
from jax.sharding import PartitionSpec as P

f32 = jnp.float32
bf16 = jnp.bfloat16
MESH = pl.DeviceIdType.MESH

gate_cap = 15.0
epsilon = 1e-06
far_below = -1e30
CONV = 3
LANES = 128
ROW_STEP = 64
NORM_STEP = 16
CONV_STEP = 32
TILE = 256
HALO = 16
SLOT = (0, 3, 1, 2)

SHAPES = {64: (8, 4, 2)}


def softcap(values):
    return gate_cap * jnp.tanh(values * (1.0 / gate_cap))


def log_one_plus(values):
    series = values * (
        1.0 + values * (-1 / 2 + values * (1 / 3 + values * (-1 / 4 + values * (1 / 5))))
    )
    return jnp.where(values < 0.015625, series, jnp.log(1.0 + values))


def log_sigmoid(values):
    return jnp.minimum(values, 0.0) - log_one_plus(jnp.exp(-jnp.abs(values)))


def normalize(values, gains):
    return values * lax.rsqrt(jnp.mean(values * values, axis=-1, keepdims=True) + epsilon) * gains


def matmul(left, right, left_dim=1, right_dim=0):
    return lax.dot_general(
        left, right, (((left_dim,), (right_dim,)), ((), ())), preferred_element_type=f32
    )


def mod(value, size):
    return lax.rem(value + size, jnp.int32(size))


def kernel(
    Z, X, C, T,
    q_in, k_in, v_in, og_in, ig_in, fg_in, res_in, mixg_in, preg_in, postg_in, gk_in, vk_in,
    outp_ref, gatep_ref, valuep_ref, downp_ref,
    out_ref,
    q_ref, k_ref, v_ref, og_ref, ig_ref, fg_ref, res_ref, mixg_ref, preg_ref, postg_ref, gk_own, vk_own,
    msend, sib_m, csend, mrecv, st_src, sib_st, cst, st_recv, ssend, srecv, nin, m_in, kwb, runc, a1, m1, d1,
    gated, wo, ushard, wu, dshard, wd, gk_ref, vk_ref, rows_all, stream, upb, hidden,
    mix_part, mix_left, mix_right, mix_top, mix_bot,
    ffn_part, ffn_left, ffn_right, ffn_top, ffn_bot,
    loc, loaded, pre, p1, p2, post, xs, xd, zs, zd, taps, ags, mss, rss, halo,
):
    NSP = Z * X * C
    rows, qk = q_ref.shape
    hv = v_ref.shape[1]
    own, D = out_ref.shape
    ffd = gatep_ref.shape[1]
    scale = float(qk) ** -0.5
    me = lax.axis_index("sp")
    tp = lax.axis_index("tp")
    core = lax.rem(me, jnp.int32(C))
    xx = lax.rem(lax.div(me, jnp.int32(C)), jnp.int32(X))
    zz = lax.div(me, jnp.int32(C * X))
    pending = []

    def at_sp(index):
        return {"sp": index, "tp": tp}

    def at_tp(index):
        return {"sp": me, "tp": index}

    def at_zx(z, x, c):
        return z * (X * C) + x * C + c

    def remote(src, dst, ssem, rsem, device):
        return pltpu.make_async_remote_copy(
            src_ref=src, dst_ref=dst, send_sem=ssem, recv_sem=rsem,
            device_id=device, device_id_type=MESH,
        )

    def send(src, dst, ssem, rsem, device):
        copy = remote(src, dst, ssem, rsem, device)
        copy.start()
        pending.append(copy)

    def send_if(condition, src, dst, ssem, rsem, device):
        copy = remote(src, dst, ssem, rsem, device)
        pl.when(condition)(copy.start)
        pending.append((condition, copy))

    def arrived(dst, ssem, rsem, device):
        remote(dst, dst, ssem, rsem, device).wait_recv()

    def ds(start, size, step=None):
        return pl.ds(pl.multiple_of(start, step or size), size)

    sibling = at_sp(me + 1 - 2 * core)

    units = lax.rem(xx + tp, jnp.int32(T))

    def holder(x):
        return {"sp": at_zx(zz, x, core), "tp": mod(tp - x, T)}

    def source(x):
        return {"sp": at_zx(zz, x, core), "tp": units}

    barrier = pltpu.get_barrier_semaphore()

    chips = NSP // C
    chip = lax.div(me, jnp.int32(C))

    def at_chip(index):
        return at_sp(index * C + core)

    def greet(p, carry):
        pl.semaphore_signal(
            barrier, 1, device_id=at_chip(mod(chip + p, chips)), device_id_type=MESH
        )
        return carry

    lax.fori_loop(1, chips, greet, 0)
    pl.semaphore_signal(barrier, 1, device_id=sibling, device_id_type=MESH)
    for k in range(1, T):
        pl.semaphore_signal(barrier, 1, device_id=at_tp(mod(tp + k, T)), device_id_type=MESH)
    for k in range(X):

        @pl.when(xx + k > 0)
        def _(k=k):
            pl.semaphore_signal(barrier, 1, device_id=source(k), device_id_type=MESH)

    loads = [
        pltpu.make_async_copy(src, dst, loaded.at[i])
        for i, (src, dst) in enumerate((
            (ig_in, ig_ref), (fg_in, fg_ref), (k_in, k_ref), (v_in, v_ref), (q_in, q_ref),
            (og_in, og_ref), (res_in, res_ref), (mixg_in, mixg_ref), (preg_in, preg_ref),
            (postg_in, postg_ref), (gk_in, gk_own), (vk_in, vk_own),
        ))
    ]
    shard = gatep_ref.shape[0]
    local = [
        pltpu.make_async_copy(gatep_ref, ushard.at[:, pl.ds(0, ffd)], loc.at[0]),
        pltpu.make_async_copy(valuep_ref, ushard.at[:, pl.ds(ffd, ffd)], loc.at[1]),
        pltpu.make_async_copy(downp_ref, dshard, loc.at[2]),
        pltpu.make_async_copy(outp_ref, wo, loc.at[3]),
    ]
    for copy in loads + local:
        copy.start()

    steps = rows // ROW_STEP
    lane = lax.broadcasted_iota(jnp.int32, (ROW_STEP, rows), 1)
    line = lax.broadcasted_iota(jnp.int32, (ROW_STEP, rows), 0)
    loads[0].wait()
    loads[1].wait()
    li_row = softcap(ig_ref[...])
    lf_row = log_sigmoid(softcap(fg_ref[...]))

    def sums(b, run_row):
        here = line + b * ROW_STEP
        run_col = jnp.sum(jnp.where(lane <= here, lf_row, 0.0), axis=1, keepdims=True)
        runc[ds(b * ROW_STEP, ROW_STEP), :] = run_col
        return run_row + jnp.sum(jnp.where(lane == here, run_col, 0.0), axis=0, keepdims=True)

    run_row = lax.fori_loop(0, steps, sums, jnp.zeros((1, rows), f32))
    total = run_row[:, rows - 1 : rows]
    lead = total - run_row + li_row
    lead_max = jnp.max(lead, axis=1, keepdims=True)
    lead_weights = jnp.exp(lead - lead_max)
    loads[2].wait()
    loads[3].wait()

    def weigh(b, normer):
        here = line + b * ROW_STEP
        at = ds(b * ROW_STEP, ROW_STEP)
        column = jnp.sum(jnp.where(lane == here, lead_weights, 0.0), axis=1, keepdims=True)
        weighted = k_ref[at, :].astype(f32) * column
        kwb[at, :] = weighted.astype(bf16)
        return normer + jnp.sum(weighted, axis=0, keepdims=True)

    normer = lax.fori_loop(0, steps, weigh, jnp.zeros((1, qk), f32))
    nq = qk // LANES
    for r in range(nq):
        st_src[r : r + 1, :] = normer[:, r * LANES : (r + 1) * LANES]
    for r in range(nq, 4):
        st_src[r : r + 1, :] = jnp.broadcast_to(total if r == nq else lead_max, (1, LANES))
    R = msend.shape[1]
    nc = hv // LANES
    for r in range(nq):
        part = matmul(kwb[:, r * LANES : (r + 1) * LANES], v_ref[...], 0, 0)
        for rr in range(LANES // R):
            for c in range(nc):
                j = (r * (LANES // R) + rr) * nc + c
                msend[j % C * chips + j // C] = part[
                    rr * R : (rr + 1) * R, c * LANES : (c + 1) * LANES
                ].astype(bf16)

    with jax.named_scope("barrier"):
        pl.semaphore_wait(barrier, chips + T - 1 + X - 1 + jnp.minimum(xx, 1))

    send(msend, sib_m, pre.at[0, 0], pre.at[1, 0], sibling)
    send(st_src, sib_st, pre.at[0, 1], pre.at[1, 1], sibling)
    is_first = core == 0
    with jax.named_scope("pair"):
        arrived(sib_st, pre.at[0, 1], pre.at[1, 1], sibling)
        arrived(sib_m, pre.at[0, 0], pre.at[1, 0], sibling)
    one = jnp.where(is_first, st_src[...], sib_st[...])
    two = jnp.where(is_first, sib_st[...], st_src[...])

    def meet(highest, following):
        decayed = highest + following[nq : nq + 1, :]
        lead_d = following[nq + 1 : nq + 2, :]
        new = jnp.maximum(decayed, lead_d)
        return new, jnp.exp(decayed - new), jnp.exp(lead_d - new)

    pair_max, weight_one, weight_two = meet(one[nq + 1 : nq + 2, :], two)
    cst[0:nq, :] = weight_one * one[0:nq, :] + weight_two * two[0:nq, :]
    cst[nq : nq + 1, :] = one[nq : nq + 1, :] + two[nq : nq + 1, :]
    cst[nq + 1 : nq + 2, :] = pair_max
    weight_mine = jnp.where(is_first, weight_one, weight_two)
    weight_sib = jnp.where(is_first, weight_two, weight_one)

    def pair(i, carry):
        for u in range(4):
            j = i * 4 + u
            csend[j] = (
                weight_mine * msend[core * chips + j].astype(f32)
                + weight_sib * sib_m[core * chips + j].astype(f32)
            ).astype(bf16)
        return carry

    lax.fori_loop(0, chips // 4, pair, 0)

    mrecv[chip] = csend[chip]
    st_recv[chip] = cst[...]

    def scatter(p, carry):
        dst = mod(chip + p, chips)
        remote(csend.at[dst], mrecv.at[chip], p1.at[0], p1.at[1], at_chip(dst)).start()
        remote(cst, st_recv.at[chip], p1.at[2], p1.at[3], at_chip(dst)).start()
        return carry

    with jax.named_scope("scatter"):
        lax.fori_loop(1, chips, scatter, 0)

    left, right, across = mod(tp - 1, T), mod(tp + 1, T), mod(tp + 2, T)
    along_y = (tp, left, right, across, at_tp)

    def block_piece(side, low, r):
        return rows_all.at[pl.ds(block_base(side) + low * half + r * part, part)]

    def ring_start(r, ks):
        for k in ks:
            low, side = ((0, 2), (1, 1), (1, 2), (0, 1))[k]
            send(
                block_piece(0, low, r), block_piece(3 - side, low, r),
                ags.at[0, r, k], ags.at[1, r, k], at_ring(ring[side]),
            )

    def ag_wait(r, k):
        with jax.named_scope("ag" + str(k)):
            side, low = ((1, 0), (2, 1), (1, 1), (2, 0), (3, 0), (3, 1))[k]
            piece = block_piece(side, low, r)
            arrived(piece, ags.at[0, r, k], ags.at[1, r, k], at_ring(fl))
            if k < 2:
                to = at_ring((fr, fl)[k])
                send(piece, block_piece(3, low, r), ags.at[0, r, k + 4], ags.at[1, r, k + 4], to)

    for copy in local:
        copy.wait()
    for copy in loads[4:]:
        copy.wait()

    def rows_of(index):
        return ds(index * shard, shard)

    weights = ((ushard, wu), (dshard, wd))
    def spread(w):
        src, dst = weights[w]
        for k in range(X):
            send_if(
                xx + k > 0, src, dst.at[rows_of(me)], xs.at[0, k, w], xs.at[1, xx, w], holder(k)
            )

    spread(0)

    @pl.when(xx == 0)
    def _():
        for src, dst in weights:
            dst[rows_of(me), :] = src[...]

    for i, (src, dst) in enumerate(((gk_own, gk_ref), (vk_own, vk_ref))):
        send_if(xx > 0, src, dst, taps.at[0, i], taps.at[1, i], at_tp(mod(tp - xx, T)))

    @pl.when(xx == 0)
    def _():
        gk_ref[...] = gk_own[...]
        vk_ref[...] = vk_own[...]

    def inside(b, carry):
        at = ds(b * ROW_STEP, ROW_STEP)
        here = line + b * ROW_STEP
        logs = jnp.where(lane <= here, runc[at, :] - run_row + li_row, far_below)
        top = jnp.max(logs, axis=1, keepdims=True)
        scores = matmul(q_ref[at, :], k_ref[...], 1, 1) * (jnp.exp(logs - top) * scale)
        m1[at, :] = top
        d1[at, :] = jnp.sum(scores, axis=1, keepdims=True)
        a1[at, :] = matmul(scores.astype(bf16), v_ref[...])
        return carry

    with jax.named_scope("inside"):
        lax.fori_loop(0, steps, inside, 0)

    def shards(w, ks):
        for k in ks:
            piece = weights[w][1].at[rows_of(at_zx(zz, k, core))]

            @pl.when(xx + k > 0)
            def _():
                arrived(piece, xs.at[0, k, w], xs.at[1, k, w], source(k))

            send(piece, piece, xd.at[0, k, w], xd.at[1, k, w], sibling)

    def shard_twins(w):
        for k in range(X):
            piece = weights[w][1].at[rows_of(at_zx(zz, k, 1 - core))]
            arrived(piece, xd.at[0, k, w], xd.at[1, k, w], sibling)

    def all_but_one(buf):
        return buf.at[pl.ds(0, chips - 1)]

    def bulk(buf, sems, s):
        remote(all_but_one(buf), all_but_one(buf), sems.at[s], sems.at[s + 1], at_sp(me)).wait()

    with jax.named_scope("p1wait"):
        bulk(mrecv, p1, 0)
        bulk(st_recv, p1, 2)

    def advance(i, state):
        highest, memory, norm = state
        for u in range(4):
            d = i * 4 + u
            ssend[d] = memory.astype(bf16)
            nin[d, 0:nq, :] = norm
            nin[d, nq : nq + 1, :] = highest
            following = st_recv[d]
            highest, before, after = meet(highest, following)
            memory = before * memory + after * mrecv[d].astype(f32)
            norm = before * norm + after * following[0:nq, :]
        return highest, memory, norm

    lax.fori_loop(
        0, chips // 4, advance,
        (jnp.full((1, LANES), far_below, f32), jnp.zeros((R, LANES), f32), jnp.zeros((nq, LANES), f32)),
    )
    part_of_core = pl.ds(core * chips, chips)
    srecv[core * chips + chip] = ssend[chip]

    def give_back(p, carry):
        dst = mod(chip + p, chips)
        remote(
            ssend.at[dst], srecv.at[core * chips + chip], p2.at[0], p2.at[1], at_chip(dst)
        ).start()
        return carry

    with jax.named_scope("giveback"):
        lax.fori_loop(1, chips, give_back, 0)

    spread(1)
    slab = shard * X * C
    ups = (at_zx(mod(zz + 1, Z), xx, core), at_zx(mod(zz - 1, Z), xx, core))

    def z_piece(w, direction, s, h, c):
        z = mod(zz - s if direction == 0 else zz + s, Z)
        return [
            weights[w][1].at[rows_of(at_zx(z, h * (X // 2) + q, c))] for q in range(X // 2)
        ]

    def z_has(direction, s, h):
        return s < Z // 2 or (s == Z // 2 and h == direction)

    def z_send(w, direction, s, h):
        if z_has(direction, s, h):
            i = (s - 1) * 2 + h
            for q, piece in enumerate(z_piece(w, direction, s - 1, h, core)):
                send(
                    piece, piece, zs.at[0, w, direction, i, q], zs.at[1, w, direction, i, q],
                    at_sp(ups[direction]),
                )

    def z_start(w, h):
        for direction in range(2):
            z_send(w, direction, 1, h)

    def z_step(w, s, h):
        with jax.named_scope(("uring", "dring")[w] + str(s) + str(h)):
            for direction in range(2):
                if z_has(direction, s, h):
                    pieces = z_piece(w, direction, s, h, core)
                    i = (s - 1) * 2 + h
                    for q, piece in enumerate(pieces):
                        arrived(
                            piece, zs.at[0, w, direction, i, q], zs.at[1, w, direction, i, q],
                            at_sp(ups[direction]),
                        )
                    z_send(w, direction, s + 1, h)
                    for q, piece in enumerate(pieces):
                        send(
                            piece, piece, zd.at[0, w, direction, i, q], zd.at[1, w, direction, i, q],
                            sibling,
                        )

    def z_twin(w, distances):
        with jax.named_scope(("utwin", "dtwin")[w]):
            for s in distances:
                for h in range(2):
                    for direction in range(2):
                        if z_has(direction, s, h):
                            i = (s - 1) * 2 + h
                            for q, piece in enumerate(z_piece(w, direction, s, h, 1 - core)):
                                arrived(
                                    piece, zd.at[0, w, direction, i, q],
                                    zd.at[1, w, direction, i, q], sibling,
                                )

    u_events = [(0, s, h) for s in range(1, Z // 2 + 1) for h in range(2)]
    d_events = [(1, s, h) for s in range(1, Z // 2 + 1) for h in range(2)]

    def z_next(events):
        if events:
            z_step(*events.pop(0))

    with jax.named_scope("ushards"):
        shards(0, range(X // 2))
    z_start(0, 0)
    with jax.named_scope("ushards2"):
        shards(0, range(X // 2, X))

    with jax.named_scope("p2wait"):
        bulk(srecv, p2, 0)
    mine = srecv.at[part_of_core]
    send(mine, mine, post.at[0], post.at[1], sibling)
    z_start(0, 1)
    with jax.named_scope("postwait"):
        other = srecv.at[pl.ds((C - 1 - core) * chips, chips)]
        arrived(other, post.at[0], post.at[1], sibling)
    stats = nin[chip]
    ahead_max, ahead_scale, sib_scale = meet(stats[nq : nq + 1, :], sib_st[...])
    ahead_max = jnp.where(is_first, stats[nq : nq + 1, :], ahead_max)
    ahead_scale = jnp.where(is_first, 1.0, ahead_scale)
    sib_scale = jnp.where(is_first, 0.0, sib_scale)
    ahead_normer = ahead_scale * stats[0:nq, :] + sib_scale * sib_st[0:nq, :]
    for j in range(NSP):
        r, c = divmod(j, nc)
        i = j % C * chips + j // C
        m_in[r * R : (r + 1) * R, c * LANES : (c + 1) * LANES] = (
            ahead_scale * srecv[i].astype(f32) + sib_scale * sib_m[i].astype(f32)
        ).astype(bf16)
    normer_in = jnp.concatenate([ahead_normer[r : r + 1, :] for r in range(nq)], axis=1)
    stab = ahead_max[:, 0:1]

    def finish(b, carry):
        at = ds(b * ROW_STEP, ROW_STEP)
        queries = q_ref[at, :]
        carried = runc[at, :] + stab
        top = m1[at, :]
        row_max = jnp.maximum(carried, top)
        inner = jnp.exp(top - row_max)
        outer = jnp.exp(carried - row_max) * scale
        reach = jnp.sum(queries.astype(f32) * normer_in, axis=1, keepdims=True)
        denominator = inner * d1[at, :] + outer * reach
        floor = jnp.maximum(jnp.abs(denominator), jnp.exp(-row_max))
        numerator = inner * a1[at, :] + outer * matmul(queries, m_in[...])
        gate = 1.0 / (1.0 + jnp.exp(-og_ref[at, :].astype(f32)))
        gated[at, :] = (numerator / floor * gate).astype(bf16)
        return carry

    half = own // 2
    part = half // 2

    class Sums:
        def __init__(self, view, base, ring, sems, summed, from_left, from_right, relay_top, relay_bot):
            self.view, self.base, self.ring, self.sems, self.summed = view, base, ring, sems, summed
            self.from_left, self.from_right = from_left, from_right
            self.relays = (relay_top, relay_bot)

        def send(self, src, dst, r, k, side):
            to = self.ring[4](self.ring[side])
            send(src, dst, self.sems.at[0, r, k], self.sems.at[1, r, k], to)

        def wait(self, dst, r, k):
            arrived(dst, self.sems.at[0, r, k], self.sems.at[1, r, k], self.ring[4](self.ring[1]))

        def piece(self, side, low, r):
            return self.view(self.summed, self.base(side) + low * half, r)

        def at_owner(self, buf, low, r):
            return self.view(buf, low * half, r)

        def far(self, r):
            for low in range(2):
                self.send(
                    self.piece(3, low, r), self.view(self.relays[low], 0, r), r, 2 + low, 2 - low
                )

        def near(self, r):
            self.send(self.piece(2, 1, r), self.at_owner(self.from_left, 1, r), r, 0, 2)
            self.send(self.piece(1, 0, r), self.at_owner(self.from_right, 0, r), r, 1, 1)

        def relay(self, r):
            for low, buf in ((0, self.from_left), (1, self.from_right)):
                relay = self.view(self.relays[low], 0, r)
                own_piece = self.piece(2 - low, low, r)
                with jax.named_scope("relay"):
                    self.wait(relay, r, 2 + low)
                if len(relay.shape) == 3:
                    steps_here = relay.shape[0]
                else:
                    steps_here = relay.shape[0] // NORM_STEP

                def merge(b, carry, relay=relay, own_piece=own_piece):
                    at = b if len(relay.shape) == 3 else ds(b * NORM_STEP, NORM_STEP)
                    relay[at] = (relay[at].astype(f32) + own_piece[at].astype(f32)).astype(bf16)
                    return carry

                lax.fori_loop(0, steps_here, merge, 0)
                self.send(relay, self.at_owner(buf, low, r), r, 4 + low, 2 - low)

        def finish(self, r):
            with jax.named_scope("sumwait"):
                self.wait(self.at_owner(self.from_left, 1, r), r, 0)
                self.wait(self.at_owner(self.from_right, 0, r), r, 1)
                self.wait(self.at_owner(self.from_left, 0, r), r, 4)
                self.wait(self.at_owner(self.from_right, 1, r), r, 5)

    def mix_view(ref, row, r):
        return ref.at[ds(row + r * part, part, 16)]

    mixes = Sums(mix_view, lambda side: along_y[side] * own, along_y, mss, mix_part, mix_left, mix_right, mix_top, mix_bot)

    def project(block):
        lines = ds(block * own, own)

        def project_tile(n, carry):
            at = ds(n * TILE, TILE)
            mix_part[lines, at] = matmul(gated[lines, :], wo[:, at]).astype(bf16)
            return carry

        with jax.named_scope("finish"):
            each = own // ROW_STEP
            lax.fori_loop(block * each, (block + 1) * each, finish, 0)
        with jax.named_scope("project"):
            lax.fori_loop(0, D // TILE, project_tile, 0)

    project(across)
    mixes.far(0)
    mixes.far(1)
    z_next(u_events)
    project(right)
    project(left)
    mixes.near(0)
    project(tp)

    def at_ring(index):
        return {
            "sp": me + core * (at_zx(zz, index, core) - me),
            "tp": index + core * (tp - index),
        }

    spot = tp + core * (xx - tp)
    fl, fr, fo = mod(spot - 1, T), mod(spot + 1, T), mod(spot + 2, T)
    ring = (spot, fl, fr, fo, at_ring)
    block_rows = own + HALO

    def block_base(block):
        return SLOT[block] * block_rows + HALO

    def join(r):
        def join_rows(b, carry):
            row = lax.rem(b, jnp.int32(part // NORM_STEP)) * NORM_STEP + r * part
            row = row + lax.div(b, jnp.int32(part // NORM_STEP)) * half
            at = ds(row, NORM_STEP)
            summed = (
                mix_part[ds(tp * own + row, NORM_STEP), :].astype(f32)
                + mix_left[at, :].astype(f32)
                + mix_right[at, :].astype(f32)
            )
            values = summed.astype(bf16).astype(f32)
            joined = (res_ref[at, :].astype(f32) + normalize(values, mixg_ref[...])).astype(bf16)
            stream[at, :] = joined
            rows_all[ds(block_base(0) + row, NORM_STEP), :] = normalize(
                joined.astype(f32), preg_ref[...]
            ).astype(bf16)
            return carry

        with jax.named_scope("join"):
            lax.fori_loop(0, 2 * (part // NORM_STEP), join_rows, 0)

    z_next(u_events)
    mixes.relay(0)
    mixes.near(1)
    z_next(u_events)
    mixes.relay(1)
    z_next(u_events)
    with jax.named_scope("dshards"):
        shards(1, range(X))
    z_next(u_events)
    z_start(1, 0)
    mixes.finish(0)
    join(0)
    ring_start(0, (0, 1, 2, 3))
    z_next(u_events)
    z_start(1, 1)
    mixes.finish(1)
    join(1)
    ring_start(1, (0, 1))

    place = me * T + tp
    after = place + 1
    is_last = after == NSP * T
    nsp = lax.rem(lax.div(after, jnp.int32(T)), jnp.int32(NSP))
    ntp = lax.rem(after, jnp.int32(T))
    ncore = lax.rem(nsp, jnp.int32(C))
    nx = lax.rem(lax.div(nsp, jnp.int32(C)), jnp.int32(X))
    nz = lax.div(nsp, jnp.int32(C * X))
    npos = ntp + ncore * (nx - ntp)
    tail_lines = pl.ds(block_base(0) + own - HALO, HALO)
    for k in range(T):
        to_sp = nsp + ncore * (at_zx(nz, k, ncore) - nsp)
        to_tp = k + ncore * (ntp - k)
        slot = mod(npos - k, T)
        to_lines = ds(slot * block_rows, HALO, 16)
        to_self = to_sp * T + to_tp == place
        go = jnp.logical_not(jnp.logical_or(is_last, to_self))
        send_if(
            go, rows_all.at[tail_lines], rows_all.at[to_lines], halo.at[0, k], halo.at[1, slot],
            {"sp": to_sp, "tp": to_tp},
        )

        @pl.when(jnp.logical_and(to_self, jnp.logical_not(is_last)))
        def _(to_lines=to_lines):
            rows_all[to_lines, :] = rows_all[tail_lines, :]

    ring_start(1, (2, 3))

    def halo_wait(slot):
        device = at_ring(mod(spot + slot, T))
        ahead = device["sp"] * T + device["tp"] - 1
        lines = pl.ds(slot * block_rows, HALO)

        @pl.when(ahead < 0)
        def _():
            rows_all[lines, :] = jnp.zeros((HALO, D), bf16)

        @pl.when(jnp.logical_and(ahead >= 0, ahead != place))
        def _():
            arrived(rows_all.at[lines], halo.at[0, 0], halo.at[1, slot], device)

    ag_wait(0, 0)
    ag_wait(0, 1)
    while u_events:
        z_next(u_events)
    z_next(d_events)
    ag_wait(1, 0)
    ag_wait(1, 1)
    z_next(d_events)

    @pl.when(xx > 0)
    def _():
        for i, dst in enumerate((gk_ref, vk_ref)):
            arrived(dst, taps.at[0, i], taps.at[1, i], at_tp(mod(tp + xx, T)))

    with jax.named_scope("shtwins"):
        shard_twins(0)
        shard_twins(1)
    z_twin(0, range(1, Z // 2 + 1))

    def mix(first, last):
        for slot in range(first, last):
            halo_wait(slot)
        lines = pl.ds(first * block_rows, (last - first) * block_rows)
        within = pl.ds(0, (last - first) * block_rows)

        def raise_tile(n, carry):
            at = ds(n * TILE, TILE)
            upb[within, at] = matmul(rows_all[lines, :], wu[:, at]).astype(bf16).astype(f32)
            return carry

        with jax.named_scope("raise"):
            lax.fori_loop(0, 2 * ffd // TILE, raise_tile, 0)
        z_next(d_events)
        windows = own // CONV_STEP

        def convolve(b, carry):
            block = lax.div(b, jnp.int32(windows))
            row = lax.rem(b, jnp.int32(windows)) * CONV_STEP
            window = ds(block * block_rows + row + HALO - 8, CONV_STEP + 8, 8)
            at = ds((first + block) * own + row, CONV_STEP)
            for c in range(0, ffd, TILE):
                both = []
                for taps_ref, start in ((gk_ref, 0), (vk_ref, ffd)):
                    block_values = upb[window, start + c : start + c + TILE]
                    summed = 0.0
                    for j in range(CONV):
                        low = 8 - CONV + 1 + j
                        summed = summed + taps_ref[j : j + 1, c : c + TILE] * block_values[low : low + CONV_STEP]
                    both.append(summed)
                hidden[at, c : c + TILE] = (both[0] / (1.0 + jnp.exp(-both[0])) * both[1]).astype(bf16)
            return carry

        with jax.named_scope("conv"):
            lax.fori_loop(0, (last - first) * windows, convolve, 0)

    zs_order = [zz]
    for d in range(1, Z // 2):
        zs_order += [mod(zz - d, Z), mod(zz + d, Z)]
    zs_order.append(mod(zz + Z // 2, Z))
    early = max(1, Z - 3)

    def lower(tile):
        at = ds(zs_order[tile] * slab, slab)
        with jax.named_scope("lower"):
            ffn_part[tile] = matmul(hidden[...], wd[at, :], 1, 1).astype(bf16)

    def ffn_view(ref, row, r):
        tiles = pl.ds(0, early) if r == 0 else pl.ds(early, Z - early)
        return ref.at[tiles, ds(row, half), :]

    ffns = Sums(ffn_view, lambda side: SLOT[side] * own, ring, rss, ffn_part, ffn_left, ffn_right, ffn_top, ffn_bot)
    mix(0, 1)
    z_next(d_events)
    for k in (2, 3, 4, 5):
        ag_wait(0, k)
    for k in (2, 3, 4, 5):
        ag_wait(1, k)
    mix(1, T)
    while d_events and d_events[0][1] <= max(0, (early - 1) // 2):
        z_next(d_events)
    for tile in range(early):
        if tile % 2 == 1:
            z_twin(1, ((tile + 1) // 2,))
        lower(tile)
    ffns.far(0)
    ffns.near(0)
    for tile in range(early, Z):
        distance = (tile + 1) // 2
        while d_events and d_events[0][1] <= distance:
            z_next(d_events)
        if tile % 2 == 1:
            z_twin(1, (distance,))
        lower(tile)
    ffns.far(1)
    ffns.relay(0)
    ffns.near(1)
    ffns.relay(1)
    ffns.finish(0)
    ffns.finish(1)

    def close(b, carry):
        at = ds(b * NORM_STEP, NORM_STEP)
        mine = ds(b * NORM_STEP, NORM_STEP)
        values, squares = [], 0.0
        for tile in range(Z):
            summed = (
                ffn_part[tile, mine, :].astype(f32)
                + ffn_left[tile, at, :].astype(f32)
                + ffn_right[tile, at, :].astype(f32)
            )
            values.append(summed.astype(bf16).astype(f32))
            squares = squares + jnp.sum(values[-1] * values[-1], axis=-1, keepdims=True)
        factor = lax.rsqrt(squares * (1.0 / D) + epsilon)
        for tile in range(Z):
            to = ds(zs_order[tile] * slab, slab)
            out_ref[at, to] = (
                stream[at, to].astype(f32) + values[tile] * factor * postg_ref[:, to]
            ).astype(bf16)
        return carry

    with jax.named_scope("close"):
        lax.fori_loop(0, own // NORM_STEP, close, 0)

    for copy in pending:
        if isinstance(copy, tuple):
            pl.when(copy[0])(copy[1].wait_send)
        else:
            copy.wait_send()


def body(
    shape,
    query_rows, key_rows, value_rows, out_gate_pre, input_gate_pre, forget_gate_pre, residual,
    out_proj, mix_gain, pre_gain, gate_proj, value_proj, gate_kernel, value_kernel, down_proj,
    post_gain,
):
    Z, X, C, T = shape
    NSP = Z * X * C
    rows, qk = query_rows.shape
    hv = value_rows.shape[1]
    own, D = residual.shape
    ffd = gate_proj.shape[1]
    R = qk * hv // LANES // NSP
    dma = pltpu.SemaphoreType.DMA
    vm = pltpu.VMEM
    inner = pl.BlockSpec(memory_space=pltpu.VMEM)
    outer = pl.BlockSpec(memory_space=pl.ANY)
    return pl.pallas_call(
        functools.partial(kernel, Z, X, C, T),
        out_shape=jax.ShapeDtypeStruct((own, D), bf16),
        in_specs=[outer] * 16,
        out_specs=inner,
        scratch_shapes=[
            vm((rows, qk), bf16),
            vm((rows, qk), bf16),
            vm((rows, hv), bf16),
            vm((rows, hv), bf16),
            vm((1, rows), f32),
            vm((1, rows), f32),
            vm((own, D), bf16),
            vm((1, D), f32),
            vm((1, D), f32),
            vm((1, D), f32),
            vm((CONV, ffd), f32),
            vm((CONV, ffd), f32),
            vm((NSP, R, LANES), bf16),
            vm((NSP, R, LANES), bf16),
            vm((NSP // C, R, LANES), bf16),
            vm((NSP // C, R, LANES), bf16),
            vm((4, LANES), f32),
            vm((4, LANES), f32),
            vm((4, LANES), f32),
            vm((NSP // C, 4, LANES), f32),
            vm((NSP // C, R, LANES), bf16),
            vm((NSP, R, LANES), bf16),
            vm((NSP // C, 4, LANES), f32),
            vm((qk, hv), bf16),
            vm((rows, qk), bf16),
            vm((rows, 1), f32),
            vm((rows, hv), f32),
            vm((rows, 1), f32),
            vm((rows, 1), f32),
            vm((rows, hv), bf16),
            vm((hv, D), bf16),
            vm((D // NSP, 2 * ffd), bf16),
            vm((D, 2 * ffd), bf16),
            vm((D // NSP, ffd), bf16),
            vm((D, ffd), bf16),
            vm((CONV, ffd), f32),
            vm((CONV, ffd), f32),
            vm((T * (own + HALO), D), bf16),
            vm((own, D), bf16),
            vm(((T - 1) * (own + HALO), 2 * ffd), f32),
            vm((rows, ffd), bf16),
        ]
        + [
            vm((rows, D), bf16),
            vm((own, D), bf16),
            vm((own, D), bf16),
            vm((own // 2, D), bf16),
            vm((own // 2, D), bf16),
            vm((Z, rows, D // Z), bf16),
            vm((Z, own, D // Z), bf16),
            vm((Z, own, D // Z), bf16),
            vm((Z, own // 2, D // Z), bf16),
            vm((Z, own // 2, D // Z), bf16),
        ]
        + [
            dma((4,)),
            dma((12,)),
            dma((2, 2)),
            dma((4,)),
            dma((2,)),
            dma((2,)),
            dma((2, X, 2)),
            dma((2, X, 2)),
            dma((2, 2, 2, Z, X // 2)),
            dma((2, 2, 2, Z, X // 2)),
            dma((2, 2)),
            dma((2, 2, 6)),
            dma((2, 2, 6)),
            dma((2, 2, 6)),
            dma((2, T)),
        ],
        compiler_params=pltpu.CompilerParams(
            collective_id=0, has_side_effects=True, vmem_limit_bytes=60 * 1024 * 1024
        ),
        name="cell_and_mixer",
    )(
        query_rows, key_rows, value_rows, out_gate_pre, input_gate_pre, forget_gate_pre, residual,
        mix_gain.reshape(1, D), pre_gain.reshape(1, D), post_gain.reshape(1, D),
        gate_kernel, value_kernel, out_proj, gate_proj, value_proj, down_proj,
    )


def solution(mesh):
    shape = (*SHAPES[mesh.shape["sp"]], mesh.shape["tp"])
    placed = (
        P("sp", "tp"),
        P("sp", "tp"),
        P("sp", "tp"),
        P("sp", "tp"),
        P("tp", "sp"),
        P("tp", "sp"),
        P(("sp", "tp"), None),
        P("tp", None),
        P(),
        P(),
        P("sp", "tp"),
        P("sp", "tp"),
        P(None, "tp"),
        P(None, "tp"),
        P("sp", "tp"),
        P(),
    )
    return jax.shard_map(
        functools.partial(body, shape), mesh=mesh, in_specs=placed,
        out_specs=P(("sp", "tp"), None), check_vma=False,
    )
```

time: 109 us -> 95.7 us (0.88)
  Pallas kernels: 107 us -> 93 us
    pallas_call x1, Pallas kernels: 107 us -> 93 us  [body(): pl.pallas_call(functools.partial(kernel, Z, X, C, T), out_shape=jax.Shape...]
where the time goes in v3:
time: 95.7 us; the launch traced here: 94.9 us
  Pallas kernels  93 us (97%)
  local copies, waits for them, and re-layouts  1.88 us (2%)
    pallas_call x1, Pallas kernels, body(): pl.pallas_call(functools.partial(kernel, Z, X, C, T), out_shape=jax.Shape...  93 us

profile of v3, /device:TPU:2, one launch (start us, length us, event | category | flops | bytes accessed | tf_op | source)
XLA Modules:
  0.0 94.9 jit_solution(9410380047812895981)
XLA Ops:
  0.0 93.0 %cell_and_mixer.1 = bf16[128,2048]{1,0:T(8,128)(2,1)} custom-call(bf16[512,256]{1,0:T(8,128)(2,1)} %q_in.1, bf16[512,256]{1,0:T(8,128)(2,1)} %k_in.1, bf16[512,512]{1,0:T(8,128)(2,1)} %v_in.1, bf16[512,512]{1,0:T(8,128)(2,1)} %og_in.1, f32[1,512]{1,0:T(1,128)} %ig_in.1, f32[1,512]{1,0:T(1,128)} %fg_in.1, bf16[128,2048]{1,0:T(8,128)(2,1)} %res_in.1, ...), custom_call_target="tpu_custom_call" | custom-call | tf_op jit(solution)/shard_map/cell_and_mixer/pallas_call | solution.py:821
  93.0 1.9 %copy.18 = bf16[128,2048]{1,0:T(8,128)(2,1)} copy(bf16[128,2048]{1,0:T(8,128)(2,1)} %cell_and_mixer.1) | data formatting | bytes 1048576

commit v4 on v3

--- a/solution.py
+++ b/solution.py
@@ -177,7 +177,7 @@
         runc[ds(b * ROW_STEP, ROW_STEP), :] = run_col
         return run_row + jnp.sum(jnp.where(lane == here, run_col, 0.0), axis=0, keepdims=True)
 
-    run_row = lax.fori_loop(0, steps, sums, jnp.zeros((1, rows), f32))
+    run_row = lax.fori_loop(0, steps, sums, jnp.zeros((1, rows), f32), unroll=True)
     total = run_row[:, rows - 1 : rows]
     lead = total - run_row + li_row
     lead_max = jnp.max(lead, axis=1, keepdims=True)
@@ -193,7 +193,7 @@
         kwb[at, :] = weighted.astype(bf16)
         return normer + jnp.sum(weighted, axis=0, keepdims=True)
 
-    normer = lax.fori_loop(0, steps, weigh, jnp.zeros((1, qk), f32))
+    normer = lax.fori_loop(0, steps, weigh, jnp.zeros((1, qk), f32), unroll=True)
     nq = qk // LANES
     for r in range(nq):
         st_src[r : r + 1, :] = normer[:, r * LANES : (r + 1) * LANES]
@@ -574,6 +574,7 @@
     project(right)
     project(left)
     mixes.near(0)
+    z_next(u_events)
     project(tp)
 
     def at_ring(index):
@@ -611,7 +612,6 @@
         with jax.named_scope("join"):
             lax.fori_loop(0, 2 * (part // NORM_STEP), join_rows, 0)
 
-    z_next(u_events)
     mixes.relay(0)
     mixes.near(1)
     z_next(u_events)
@@ -702,7 +702,11 @@
             return carry
 
         with jax.named_scope("raise"):
-            lax.fori_loop(0, 2 * ffd // TILE, raise_tile, 0)
+            lax.fori_loop(0, ffd // TILE, raise_tile, 0)
+        if first > 0:
+            z_next(d_events)
+        with jax.named_scope("raise"):
+            lax.fori_loop(ffd // TILE, 2 * ffd // TILE, raise_tile, 0)
         z_next(d_events)
         windows = own // CONV_STEP
 
@@ -732,10 +736,15 @@
     zs_order.append(mod(zz + Z // 2, Z))
     early = max(1, Z - 3)
 
-    def lower(tile):
-        at = ds(zs_order[tile] * slab, slab)
+    def lower(first, last):
+        def lower_tile(tile, carry):
+            away = lax.div(tile + 1, jnp.int32(2)) * (1 - 2 * lax.rem(tile, jnp.int32(2)))
+            z = lax.rem(zz + away + Z, jnp.int32(Z))
+            ffn_part[tile] = matmul(hidden[...], wd[ds(z * slab, slab), :], 1, 1).astype(bf16)
+            return carry
+
         with jax.named_scope("lower"):
-            ffn_part[tile] = matmul(hidden[...], wd[at, :], 1, 1).astype(bf16)
+            lax.fori_loop(first, last, lower_tile, 0)
 
     def ffn_view(ref, row, r):
         tiles = pl.ds(0, early) if r == 0 else pl.ds(early, Z - early)
@@ -751,19 +760,17 @@
     mix(1, T)
     while d_events and d_events[0][1] <= max(0, (early - 1) // 2):
         z_next(d_events)
-    for tile in range(early):
-        if tile % 2 == 1:
-            z_twin(1, ((tile + 1) // 2,))
-        lower(tile)
+    z_twin(1, range(1, (early - 1) // 2 + 1))
+    lower(0, early)
     ffns.far(0)
     ffns.near(0)
-    for tile in range(early, Z):
-        distance = (tile + 1) // 2
-        while d_events and d_events[0][1] <= distance:
-            z_next(d_events)
-        if tile % 2 == 1:
-            z_twin(1, (distance,))
-        lower(tile)
+    while d_events:
+        z_next(d_events)
+    if early < Z - 1:
+        z_twin(1, range((early - 1) // 2 + 1, Z // 2))
+        lower(early, Z - 1)
+    z_twin(1, (Z // 2,))
+    lower(Z - 1, Z)
     ffns.far(1)
     ffns.relay(0)
     ffns.near(1)

time: 95.7 us -> 94.7 us (0.990)
  no operation moved by 1% of the time
where the time goes in v4:
time: 94.7 us; the launch traced here: 94.6 us
  Pallas kernels  92.7 us (98%)
  local copies, waits for them, and re-layouts  1.88 us (2%)
    pallas_call x1, Pallas kernels, body(): pl.pallas_call(functools.partial(kernel, Z, X, C, T), out_shape=jax.Shape...  92.7 us

profile of v4, /device:TPU:2, one launch (start us, length us, event | category | flops | bytes accessed | tf_op | source)
XLA Modules:
  0.0 94.6 jit_solution(2440526639029643971)
XLA Ops:
  0.0 92.7 %cell_and_mixer.1 = bf16[128,2048]{1,0:T(8,128)(2,1)} custom-call(bf16[512,256]{1,0:T(8,128)(2,1)} %q_in.1, bf16[512,256]{1,0:T(8,128)(2,1)} %k_in.1, bf16[512,512]{1,0:T(8,128)(2,1)} %v_in.1, bf16[512,512]{1,0:T(8,128)(2,1)} %og_in.1, f32[1,512]{1,0:T(1,128)} %ig_in.1, f32[1,512]{1,0:T(1,128)} %fg_in.1, bf16[128,2048]{1,0:T(8,128)(2,1)} %res_in.1, ...), custom_call_target="tpu_custom_call" | custom-call | tf_op jit(solution)/shard_map/cell_and_mixer/pallas_call | solution.py:828
  92.7 1.9 %copy.18 = bf16[128,2048]{1,0:T(8,128)(2,1)} copy(bf16[128,2048]{1,0:T(8,128)(2,1)} %cell_and_mixer.1) | data formatting | bytes 1048576

commit v5 on v4

--- a/solution.py
+++ b/solution.py
@@ -673,11 +673,12 @@
 
     ag_wait(0, 0)
     ag_wait(0, 1)
-    while u_events:
-        z_next(u_events)
+    z_next(u_events)
     z_next(d_events)
     ag_wait(1, 0)
     ag_wait(1, 1)
+    while u_events:
+        z_next(u_events)
     z_next(d_events)
 
     @pl.when(xx > 0)
@@ -703,11 +704,11 @@
 
         with jax.named_scope("raise"):
             lax.fori_loop(0, ffd // TILE, raise_tile, 0)
+        z_next(d_events)
+        with jax.named_scope("raise"):
+            lax.fori_loop(ffd // TILE, 2 * ffd // TILE, raise_tile, 0)
         if first > 0:
             z_next(d_events)
-        with jax.named_scope("raise"):
-            lax.fori_loop(ffd // TILE, 2 * ffd // TILE, raise_tile, 0)
-        z_next(d_events)
         windows = own // CONV_STEP
 
         def convolve(b, carry):
@@ -827,7 +828,7 @@
     outer = pl.BlockSpec(memory_space=pl.ANY)
     return pl.pallas_call(
         functools.partial(kernel, Z, X, C, T),
-        out_shape=jax.ShapeDtypeStruct((own, D), bf16),
+        out_shape=pltpu.VMEM((own, D), bf16),
         in_specs=[outer] * 16,
         out_specs=inner,
         scratch_shapes=[

time: 94.7 us -> 92.3 us (0.975)
  Pallas kernels: 92.7 us -> 91.4 us
  local copies, waits for them, and re-layouts: 1.88 us -> 0.8 us
    pallas_call x1, Pallas kernels: 92.7 us -> 91.4 us  [body(): pl.pallas_call(functools.partial(kernel, Z, X, C, T), out_shape=pltpu.VME...]
    unnamed x1, local copies, waits for them, and re-layouts: 1.88 us -> 0.8 us
where the time goes in v5:
time: 92.3 us; the launch traced here: 92.2 us
  Pallas kernels  91.4 us (99%)
    pallas_call x1, Pallas kernels, body(): pl.pallas_call(functools.partial(kernel, Z, X, C, T), out_shape=pltpu.VME...  91.4 us

profile of v5, /device:TPU:2, one launch (start us, length us, event | category | flops | bytes accessed | tf_op | source)
XLA Modules:
  0.0 92.2 jit_solution(5662417412327086321)
XLA Ops:
  0.0 91.4 %cell_and_mixer.1 = bf16[128,2048]{1,0:T(8,128)(2,1)S(1)} custom-call(bf16[512,256]{1,0:T(8,128)(2,1)} %q_in.1, bf16[512,256]{1,0:T(8,128)(2,1)} %k_in.1, bf16[512,512]{1,0:T(8,128)(2,1)} %v_in.1, bf16[512,512]{1,0:T(8,128)(2,1)} %og_in.1, f32[1,512]{1,0:T(1,128)} %ig_in.1, f32[1,512]{1,0:T(1,128)} %fg_in.1, bf16[128,2048]{1,0:T(8,128)(2,1)} %res_in.1, ...), custom_call_target="tpu_custom_call" | custom-call | tf_op jit(solution)/shard_map/cell_and_mixer/pallas_call | solution.py:829
  91.4 0.8 copy.18

commit v6 on v5

--- a/solution.py
+++ b/solution.py
@@ -610,7 +610,7 @@
             return carry
 
         with jax.named_scope("join"):
-            lax.fori_loop(0, 2 * (part // NORM_STEP), join_rows, 0)
+            lax.fori_loop(0, 2 * (part // NORM_STEP), join_rows, 0, unroll=2)
 
     mixes.relay(0)
     mixes.near(1)
@@ -800,7 +800,7 @@
         return carry
 
     with jax.named_scope("close"):
-        lax.fori_loop(0, own // NORM_STEP, close, 0)
+        lax.fori_loop(0, own // NORM_STEP, close, 0, unroll=2)
 
     for copy in pending:
         if isinstance(copy, tuple):

time: 92.3 us -> 91.9 us (level)
  no operation moved by 1% of the time
where the time goes in v6:
time: 91.9 us; the launch traced here: 91.8 us
  Pallas kernels  91 us (99%)
    pallas_call x1, Pallas kernels, body(): pl.pallas_call(functools.partial(kernel, Z, X, C, T), out_shape=pltpu.VME...  91 us

profile of v6, /device:TPU:2, one launch (start us, length us, event | category | flops | bytes accessed | tf_op | source)
XLA Modules:
  0.0 91.8 jit_solution(17740435723866207769)
XLA Ops:
  0.0 91.0 %cell_and_mixer.1 = bf16[128,2048]{1,0:T(8,128)(2,1)S(1)} custom-call(bf16[512,256]{1,0:T(8,128)(2,1)} %q_in.1, bf16[512,256]{1,0:T(8,128)(2,1)} %k_in.1, bf16[512,512]{1,0:T(8,128)(2,1)} %v_in.1, bf16[512,512]{1,0:T(8,128)(2,1)} %og_in.1, f32[1,512]{1,0:T(1,128)} %ig_in.1, f32[1,512]{1,0:T(1,128)} %fg_in.1, bf16[128,2048]{1,0:T(8,128)(2,1)} %res_in.1, ...), custom_call_target="tpu_custom_call" | custom-call | tf_op jit(solution)/shard_map/cell_and_mixer/pallas_call | solution.py:829
  91.0 0.8 copy.18
